TPU v7x, 256 devices: a whole 4x4x8 slice. The times are simulated.
256 devices in a mesh: sp: 64 (over z, y, core), tp: 4 (over x).
Axes of the slice: x: 4, y: 4, z: 8, core: 2. Of those that a mesh axis runs over, the one named last changes fastest.
Arguments:
- mixer_input: bfloat16 [16384, 1024], P('sp', 'tp'), may hold values from -6 to 6
- retention: float32 [64, 16384], P('tp', 'sp'), may hold values from -1 to 0
- decay_real: float32 [64, 64], P('tp'), may hold values from -0.7 to -0.3
- decay_freq: float32 [64, 64], P('tp'), may hold values from 0 to 26
- log_step: float32 [64], P('tp')
- input_real: float32 [64, 64, 16], P('tp')
- input_imag: float32 [64, 64, 16], P('tp')
- readout_real: float32 [64, 16, 64], P('tp'), may hold values from -0.5 to 0.5
- readout_imaginary: float32 [64, 16, 64], P('tp'), may hold values from -0.5 to 0.5
- skip_weight: float32 [64, 16], P('tp'), may hold values from -4 to 4
- norm_gain: float32 [1024], replicated, may hold values from 0.1 to 1.9
- projection: bfloat16 [1024, 2048], P('tp'), may hold values from -0.1875 to 0.1875
- residual: bfloat16 [16384, 2048], P(('sp', 'tp')), may hold values from -6 to 6
- mix_gain: float32 [2048], replicated, may hold values from 0.1 to 1.9
- routes: int32 [16384, 2], P(('sp', 'tp')), may hold values from 0 to 63, all different within a row; in each aligned block of 64 rows (0 to 63, 64 to 127, ...) at most 4 rows name the same one
- route_weight: float32 [16384, 2], P(('sp', 'tp')), may hold values from 0.5 to 2
- expert_gate: bfloat16 [64, 2048, 512], P('sp'), may hold values from -0.125 to 0.125
- expert_up: bfloat16 [64, 2048, 512], P('sp'), may hold values from -0.125 to 0.125
- expert_down: bfloat16 [64, 512, 2048], P('sp'), may hold values from -0.25 to 0.25
- final_gain: float32 [2048], replicated, may hold values from 0.1 to 1.9
Outputs:
- layer_out: bfloat16 [16384, 2048], P(('sp', 'tp'))
Inputs may be any that keep to these rules, and one draw needn't show every extreme that they name: `routes`: in each aligned block of 64 rows no expert is named by more than 4 rows, and in some blocks one is named by exactly 4 rows; each row names 2 different experts.
All inputs are finite; a program needn't handle non-finite values.
Results may differ from a plain program's by a relative error of at most 0.017.
Values may be sent and summed in bfloat16 or wider, within the bound.
A program may use at most 64 MiB of HBM per device.

v0:
```python
import jax
import jax.numpy as jnp
from jax import lax
from jax.sharding import PartitionSpec as P

PICKS = 2
MIX_WIDTH = 1024


deep_alpha = 2.0**0.25
span_length = 16


def copy_for_each(x, axis):
    copies = jnp.broadcast_to(x, (lax.axis_size(axis), *x.shape))
    return lax.all_to_all(copies, axis, split_axis=0, concat_axis=0, tiled=True)


def gathered_once(x, axis):
    leaves = jax.tree.leaves(x)
    sequence = sorted(range(len(leaves)), key=lambda k: -leaves[k].size)
    width = (1, *leaves[sequence[0]].shape)[-1]
    lines = [
        jnp.pad(leaves[k].reshape(-1), (0, -leaves[k].size % width)).reshape(-1, width)
        for k in sequence
    ]
    both, at, found = (copy_for_each(jnp.concatenate(lines), axis), 0, {})
    for k, line in zip(sequence, lines):
        piece = both[:, at : at + len(line)].reshape(len(both), -1)
        found[k] = piece[:, : leaves[k].size].reshape(-1, *leaves[k].shape)
        at += len(line)
    numbers = iter(range(len(leaves)))
    return jax.tree.map(lambda _: found[next(numbers)], x)


def combined_pairwise(pieces, combine):
    while len(jax.tree.leaves(pieces)[0]) > 1:
        pieces = jax.vmap(combine)(
            *(jax.tree.map(lambda part: part[side::2], pieces) for side in (0, 1))
        )
    return jax.tree.map(lambda part: part[0], pieces)


def entering(x, axis, combine, identity):
    devices, here = (lax.axis_size(axis), lax.axis_index(axis))
    passed = jnp.arange(devices) < here

    def kept(part, zero, own):
        part = jnp.where(
            passed.reshape(-1, *(1 for _ in own.shape)), part, jnp.asarray(zero, own.dtype)
        )
        return part

    pieces = gathered_once(x, axis)
    return combined_pairwise(jax.tree.map(kept, pieces, identity, x), combine)


def input_factor(decay_real, decay_freq, log_step):
    stride = jnp.exp(log_step)[:, None]
    growth = decay_real * stride
    turning = decay_freq * stride
    upper_real = jnp.expm1(growth) * jnp.cos(turning) - 2.0 * jnp.sin(0.5 * turning) ** 2
    upper_imag = jnp.exp(growth) * jnp.sin(turning)
    denominator = decay_real * decay_real + decay_freq * decay_freq
    factor_real = (upper_real * decay_real + upper_imag * decay_freq) / denominator
    factor_imag = (upper_imag * decay_real - upper_real * decay_freq) / denominator
    return (growth, turning, factor_real, factor_imag)


def layer_norm(values, scales):
    centered = values - jnp.mean(values, axis=-1, keepdims=True)
    variance = jnp.mean(centered * centered, axis=-1, keepdims=True)
    return centered * lax.rsqrt(variance + 1e-05) * scales


def chain_combine(earlier, later):
    return (
        earlier[0] * later[0] - earlier[1] * later[1],
        earlier[0] * later[1] + earlier[1] * later[0],
        later[0] * earlier[2] - later[1] * earlier[3] + later[2],
        later[0] * earlier[3] + later[1] * earlier[2] + later[3],
    )


def times_complex(left_real, left_imag, right_real, right_imag):
    return (
        left_real * right_real - left_imag * right_imag,
        left_real * right_imag + left_imag * right_real,
    )


def read_state(state_real_part, state_imaginary, readout_real, readout_imaginary):
    leading_term = jnp.einsum("motx,tkx->motk", state_real_part, readout_real)
    return leading_term - jnp.einsum("motx,tkx->motk", state_imaginary, readout_imaginary)


def local(
    mixer_input,
    retention,
    decay_real,
    decay_freq,
    log_step,
    input_real,
    input_imag,
    readout_real,
    readout_imaginary,
    skip_weight,
    norm_gain,
    projection,
    residual,
    mix_gain,
    routes,
    route_weight,
    expert_gate,
    expert_up,
    expert_down,
    final_gain,
):
    token_count = mixer_input.shape[0]
    group_count = decay_real.shape[0]
    channel_count = input_real.shape[2]
    span_count = token_count // span_length
    growth, turning, factor_real, factor_imag = input_factor(decay_real, decay_freq, log_step)
    bar_real = factor_real[:, :, None] * input_real - factor_imag[:, :, None] * input_imag
    bar_imag = factor_real[:, :, None] * input_imag + factor_imag[:, :, None] * input_real
    inputs = mixer_input.astype(jnp.float32).reshape(token_count, group_count, channel_count)
    drive_real = jnp.einsum("tgc,gpc->tgp", inputs, bar_real)
    drive_imag = jnp.einsum("tgc,gpc->tgp", inputs, bar_imag)
    drive_real = drive_real.reshape(span_count, span_length, group_count, -1)
    drive_imag = drive_imag.reshape(span_count, span_length, group_count, -1)
    held_log = jnp.cumsum(
        jnp.transpose(retention).reshape(span_count, span_length, group_count), axis=1
    )
    offsets = jnp.arange(1, span_length + 1, dtype=jnp.float32)[:, None, None]
    log_size = offsets * growth + held_log[:, :, :, None]
    turn_angle = offsets * turning
    grown_size = jnp.exp(log_size)
    shrunk = jnp.exp(-log_size)
    prefix_real = grown_size * jnp.cos(turn_angle)
    prefix_imag = grown_size * jnp.sin(turn_angle)
    weighted_real, weighted_imag = times_complex(
        drive_real, drive_imag, shrunk * jnp.cos(turn_angle), -shrunk * jnp.sin(turn_angle)
    )
    inner_real, inner_imag = times_complex(
        prefix_real,
        prefix_imag,
        jnp.cumsum(weighted_real, axis=1),
        jnp.cumsum(weighted_imag, axis=1),
    )
    scanned = lax.associative_scan(
        chain_combine,
        (prefix_real[:, -1], prefix_imag[:, -1], inner_real[:, -1], inner_imag[:, -1]),
        axis=0,
    )
    ones_row = jnp.ones_like(scanned[0][:1])
    zeros_row = jnp.zeros_like(ones_row)
    enter_decay_real = jnp.concatenate([ones_row, scanned[0][:-1]], axis=0)
    enter_decay_imag = jnp.concatenate([zeros_row, scanned[1][:-1]], axis=0)
    enter_state_real = jnp.concatenate([zeros_row, scanned[2][:-1]], axis=0)
    enter_state_imag = jnp.concatenate([zeros_row, scanned[3][:-1]], axis=0)
    identity = (
        jnp.ones_like(growth),
        jnp.zeros_like(growth),
        jnp.zeros_like(growth),
        jnp.zeros_like(growth),
    )
    carried = entering(
        (scanned[0][-1], scanned[1][-1], scanned[2][-1], scanned[3][-1]),
        "sp",
        chain_combine,
        identity,
    )
    skip_term = (skip_weight * inputs).reshape(span_count, span_length, group_count, channel_count)
    carry_real, carry_imag = times_complex(
        enter_decay_real, enter_decay_imag, carried[2], carried[3]
    )
    state_real_part, state_imaginary = times_complex(
        prefix_real,
        prefix_imag,
        (enter_state_real + carry_real)[:, None],
        (enter_state_imag + carry_imag)[:, None],
    )
    readout_result = read_state(
        inner_real + state_real_part, inner_imag + state_imaginary, readout_real, readout_imaginary
    )
    mixed_seq = (
        jax.nn.gelu(readout_result + skip_term).astype(jnp.bfloat16).reshape(token_count, -1)
    )
    row_count = token_count // lax.axis_size("tp")
    whole_rows = lax.all_to_all(mixed_seq, "tp", split_axis=0, concat_axis=1, tiled=True)
    whole_float = whole_rows.astype(jnp.float32)
    squares = jnp.sum(whole_float * whole_float, axis=1)
    scaled = (whole_float * norm_gain).astype(jnp.bfloat16)
    summed = jnp.dot(
        scaled,
        lax.all_gather(projection, "tp", axis=0, tiled=True),
        preferred_element_type=jnp.float32,
    )
    mix = summed * lax.rsqrt(squares / MIX_WIDTH + 1e-06)[:, None]
    hidden = layer_norm(deep_alpha * residual.astype(jnp.float32) + mix, mix_gain).astype(
        jnp.bfloat16
    )
    expert_count = lax.axis_size("sp")
    capacity = max(2, 2 * row_count * PICKS // expert_count)
    chosen = routes.reshape(-1)
    onehot = (chosen[:, None] == jnp.arange(expert_count, dtype=jnp.int32)[None, :]).astype(
        jnp.int32
    )
    slot_index = jnp.sum((jnp.cumsum(onehot, axis=0) - 1) * onehot, axis=1)
    target = chosen * capacity + slot_index
    source_row = jnp.full((expert_count * capacity,), row_count, jnp.int32)
    source_row = source_row.at[target].set(jnp.arange(row_count * PICKS, dtype=jnp.int32) // PICKS)
    padded = jnp.concatenate([hidden, jnp.zeros((1, hidden.shape[1]), hidden.dtype)], axis=0)
    outgoing = padded[source_row].reshape(expert_count, capacity, -1)
    received = lax.all_to_all(outgoing, "sp", split_axis=0, concat_axis=0, tiled=True)
    arrived = received.reshape(-1, received.shape[2])
    gate_act = jnp.dot(arrived, expert_gate[0], preferred_element_type=jnp.float32)
    up_act = jnp.dot(arrived, expert_up[0], preferred_element_type=jnp.float32)
    active = (jax.nn.silu(gate_act) * up_act).astype(jnp.bfloat16)
    produced = jnp.dot(active, expert_down[0], preferred_element_type=jnp.float32).astype(
        jnp.bfloat16
    )
    returned = lax.all_to_all(
        produced.reshape(received.shape), "sp", split_axis=0, concat_axis=0, tiled=True
    )
    gathered_rows = returned.reshape(expert_count * capacity, -1)[target].reshape(
        row_count, PICKS, -1
    )
    expert_mix = jnp.sum(route_weight[:, :, None] * gathered_rows.astype(jnp.float32), axis=1)
    layer_out = layer_norm(deep_alpha * hidden.astype(jnp.float32) + expert_mix, final_gain)
    return layer_out.astype(jnp.bfloat16)


def solution(mesh):
    in_specs = (
        P("sp", "tp"),
        P("tp", "sp"),
        P("tp", None),
        P("tp", None),
        P("tp"),
        P("tp", None, None),
        P("tp", None, None),
        P("tp", None, None),
        P("tp", None, None),
        P("tp", None),
        P(),
        P("tp", None),
        P(("sp", "tp"), None),
        P(),
        P(("sp", "tp"), None),
        P(("sp", "tp"), None),
        P("sp", None, None),
        P("sp", None, None),
        P("sp", None, None),
        P(),
    )
    out_specs = P(("sp", "tp"), None)
    return jax.shard_map(local, mesh=mesh, in_specs=in_specs, out_specs=out_specs, check_vma=False)
```

profile of v0, /device:TPU:1, one launch (start us, length us, event | category | flops | bytes accessed | tf_op | source)
XLA Modules:
  0.0 254.9 jit_solution(14501711055475879677)
XLA Ops:
  9.2 2.3 convolution_bitcast_fusion.1
  13.3 3.7 %copy.39 = f32[256,16,64]{2,1,0:T(8,128)} copy(f32[256,16,64]{0,2,1:T(8,128)} %convolution_bitcast_fusion.1) | data formatting | bytes 2097152 | tf_op jit(solution)/shard_map/tgc,gpc->tgp/transpose | solution.py:127
  17.1 2.5 copy.40
  21.8 2.8 %fusion.23 = f32[16,16,16,64]{3,2,1,0:T(8,128)S(1)} fusion(f32[16,16,16,64]{3,2,1,0:T(8,128)} %bitcast.107, f32[16,16,16,64]{3,2,1,0:T(8,128)} %bitcast.109, f32[16,16,64]{2,1,0:T(8,128)S(1)} %get-tuple-element.90, f32[16,16,64]{2,1,0:T(8,128)S(1)} %get-tuple-element.89, f32[16,16,16]{2,1,0:T(8,128)S(1)} %copy.37, f32[16,16,64]{2,1,0:T(8,128)S(1)} %get-tuple-element.93), kind=kOutput, calls=%fused_computation.31 | output fusion | flops 6029312 | bytes 3358720 | tf_op jit(solution)/shard_map/jit(cumsum)/reduce_window_sum | solution.py:147
  45.0 2.9 %pad.274 = f32[16,16,64]{2,1,0:T(8,128)S(1)} pad(f32[8,16,64]{2,1,0:T(8,128)} %add.453, f32[]{:T(128)} %constant.29.clone.1), padding=1_0_1x0_0_0x0_0_0 | pad | bytes 98308
  51.5 3.4 %reshape.196 = f32[64,1,4096]{2,1,0:T(1,128)} reshape(f32[64,64,64]{2,1,0:T(8,128)} %broadcast_in_dim.33) | data formatting | bytes 2097152
  55.0 13.2 %all-to-all-start = ((f32[64,1,4096]{2,1,0:T(1,128)}), f32[64,1,4096]{2,1,0:T(1,128)S(1)}, u32[]{:S(2)}, u32[]{:S(2)}) async-start(f32[64,1,4096]{2,1,0:T(1,128)} %reshape.196), calls=%async_computation | async-start | bytes 2097152 | tf_op jit(solution)/shard_map/all_to_all | solution.py:16
  72.6 4.7 %pad.177 = f32[15,16,64]{2,1,0:T(8,128)} pad(f32[8,16,64]{2,1,0:T(8,128)} %copy-done.19, f32[]{:T(128)} %constant.29.clone.1), padding=0_0_1x0_0_0x0_0_0 | pad | bytes 94212 | tf_op jit(solution)/shard_map/slice | solution.py:160
  77.2 4.7 %pad.132 = f32[16,16,64]{2,1,0:T(8,128)} pad(f32[8,16,64]{2,1,0:T(8,128)} %copy-done.16, f32[]{:T(128)} %constant.29.clone.1), padding=1_0_1x0_0_0x0_0_0 | pad | bytes 98308 | tf_op jit(solution)/shard_map/pad | solution.py:150
  81.9 4.7 %pad.175 = f32[15,16,64]{2,1,0:T(8,128)} pad(f32[8,16,64]{2,1,0:T(8,128)} %copy-done.18, f32[]{:T(128)} %constant.29.clone.1), padding=0_0_1x0_0_0x0_0_0 | pad | bytes 94212 | tf_op jit(solution)/shard_map/slice | solution.py:158
  86.6 4.7 %pad.118 = f32[16,16,64]{2,1,0:T(8,128)} pad(f32[8,16,64]{2,1,0:T(8,128)} %copy-done.17, f32[]{:T(128)} %constant.29.clone.1), padding=1_0_1x0_0_0x0_0_0 | pad | bytes 98308 | tf_op jit(solution)/shard_map/pad | solution.py:150
  91.2 2.9 %reshape.164 = f32[16,16,16,16]{3,2,1,0:T(8,128)} reshape(bf16[256,256]{1,0:T(8,128)(2,1)} %param.20) | data formatting | bytes 393216 | tf_op jit(solution)/shard_map/reshape | solution.py:126
  94.1 4.7 %pad.131 = f32[16,16,64]{2,1,0:T(8,128)} pad(f32[8,16,64]{2,1,0:T(8,128)} %pad_maximum_fusion.1, f32[]{:T(128)} %constant.29.clone.1), padding=0_1_1x0_0_0x0_0_0 | pad | bytes 98308 | tf_op jit(solution)/shard_map/pad | solution.py:150
  98.8 4.7 %pad.117 = f32[16,16,64]{2,1,0:T(8,128)} pad(f32[8,16,64]{2,1,0:T(8,128)} %pad_maximum_fusion, f32[]{:T(128)} %constant.29.clone.1), padding=0_1_1x0_0_0x0_0_0 | pad | bytes 98308 | tf_op jit(solution)/shard_map/pad | solution.py:150
  111.2 1.6 slice_add_fusion.37
  112.9 1.6 slice_add_fusion.36
  119.2 4.4 %reduce.2 = f32[64,4096]{1,0:T(8,128)S(1)} reduce(f32[64,1,4096]{2,1,0:T(1,128)} %copy-done.9, f32[]{:T(128)} %broadcast.265), dimensions={1}, to_apply=%all_to_all.19.reduce_sub_computation | reduce | bytes 2097156 | tf_op jit(solution)/shard_map/all_to_all | solution.py:16
  123.6 2.2 reshape.197
  125.8 1.7 slice_select_fusion.3
  135.0 1.7 all_to_all.20
  136.7 4.0 %all-to-all-start.1 = ((bf16[4,64,256]{2,1,0:T(8,128)(2,1)}), bf16[4,64,256]{2,1,0:T(8,128)(2,1)S(1)}, u32[]{:S(2)}, u32[]{:S(2)}) async-start(bf16[4,64,256]{2,1,0:T(8,128)(2,1)} %all_to_all.20), calls=%async_computation.1 | async-start | bytes 262144 | tf_op jit(solution)/shard_map/all_to_all | solution.py:190
  140.7 4.8 %all-to-all-done.1 = bf16[4,64,256]{2,1,0:T(8,128)(2,1)S(1)} async-done(((bf16[4,64,256]{2,1,0:T(8,128)(2,1)}), bf16[4,64,256]{2,1,0:T(8,128)(2,1)S(1)}, u32[]{:S(2)}, u32[]{:S(2)}) %all-to-all-start.1) | async-done | bytes 131104 | tf_op jit(solution)/shard_map/all_to_all | solution.py:190
  145.7 3.2 %fusion.103 = (f32[64]{0:T(128)S(1)}, f32[64,2048]{1,0:T(8,128)S(1)}) fusion(f32[64]{0:T(128)S(1)} %add_rsqrt_fusion.2, bf16[1024,2048]{1,0:T(8,128)(2,1)} %all-gather.2.cloned.1.call-done, f32[64,1024]{1,0:T(8,128)S(1)} %bitcast.113, f32[1024]{0:T(1024)S(1)} %copy-done.36, bf16[64,2048]{1,0:T(8,128)(2,1)S(1)} %copy-done.26), kind=kOutput, calls=%fused_computation.241 | convolution fusion | flops 269221824 | bytes 5247488 | tf_op jit(solution)/shard_map/dot_general | solution.py:194
  152.5 39.9 %all_to_all.28 = bf16[64,4,2048]{2,1,0:T(4,128)(2,1)S(1)} all-to-all(bf16[64,4,2048]{2,1,0:T(4,128)(2,1)} %reshape.159), channel_id=1, replica_groups=mesh['sp'=64,'tp'=4] {'sp'}, dimensions={0} | all-to-all | bytes 2097152 | tf_op jit(solution)/shard_map/all_to_all | solution.py:215
  193.5 3.5 %fusion.44 = f32[256,512]{1,0:T(8,128)} fusion(bf16[256,2048]{1,0:T(8,128)(2,1)} %reshape.160, bf16[1,2048,512]{2,1,0:T(8,128)(2,1)} %param.36), kind=kOutput, calls=%fused_computation.48 | convolution fusion | flops 536870912 | bytes 3670016 | tf_op jit(solution)/shard_map/dot_general | solution.py:217
  197.0 4.0 %convolution_convert_fusion = bf16[256,2048]{1,0:T(8,128)(2,1)} fusion(bf16[1,512,2048]{2,1,0:T(8,128)(2,1)S(1)} %copy-done, bf16[256,2048]{1,0:T(8,128)(2,1)S(1)} %copy-done.15, bf16[1,2048,512]{2,1,0:T(8,128)(2,1)} %param.37, f32[256,512]{1,0:T(8,128)} %fusion.44), kind=kOutput, calls=%fused_computation.16 | convolution fusion | flops 1075052544 | bytes 6815744 | tf_op jit(solution)/shard_map/dot_general | solution.py:220
  201.0 2.3 reshape.161
  203.2 6.5 %all-to-all-start.3 = ((bf16[64,4,2048]{2,1,0:T(4,128)(2,1)}), bf16[64,4,2048]{2,1,0:T(4,128)(2,1)}, u32[]{:S(2)}, u32[]{:S(2)}) async-start(bf16[64,4,2048]{2,1,0:T(4,128)(2,1)} %reshape.161), calls=%async_computation.3 | async-start | bytes 2097152 | tf_op jit(solution)/shard_map/all_to_all | solution.py:223
  209.8 28.0 %all-to-all-done.3 = bf16[64,4,2048]{2,1,0:T(4,128)(2,1)} async-done(((bf16[64,4,2048]{2,1,0:T(4,128)(2,1)}), bf16[64,4,2048]{2,1,0:T(4,128)(2,1)}, u32[]{:S(2)}, u32[]{:S(2)}) %all-to-all-start.3) | async-done | bytes 1048608 | tf_op jit(solution)/shard_map/all_to_all | solution.py:223
  239.1 1.7 gather_fusion.1
  240.9 2.7 %reshape.166 = f32[64,2,2048]{2,1,0:T(2,128)} reshape(bf16[128,2048]{1,0:T(8,128)(2,1)} %gather_fusion.1) | data formatting | bytes 1572864 | tf_op jit(solution)/shard_map/convert_element_type | solution.py:229
  243.6 2.8 %multiply_reduce_fusion = f32[64,2048]{1,0:T(8,128)S(1)} fusion(f32[64,2,2048]{2,1,0:T(2,128)} %reshape.166, f32[64,2]{1,0:T(8,128)S(1)} %copy.48), kind=kLoop, calls=%fused_computation.60 | loop fusion | flops 393216 | bytes 1573376 | tf_op jit(solution)/shard_map/reduce_sum | solution.py:229
  (217 shorter events, 62.3 us)
Async XLA Ops:
  6.5 190.4 %copy-start = (bf16[1,512,2048]{2,1,0:T(8,128)(2,1)S(1)}, bf16[1,512,2048]{2,1,0:T(8,128)(2,1)}, u32[]{:S(2)}) copy-start(bf16[1,512,2048]{2,1,0:T(8,128)(2,1)} %param.38) | copy-start | bytes 6291460
  17.1 2.5 copy-start.34
  21.7 2.8 %copy-start.10 = (f32[16,16,64]{2,1,0:T(8,128)}, f32[16,16,64]{2,1,0:T(8,128)S(1)}, u32[]{:S(2)}) copy-start(f32[16,16,64]{2,1,0:T(8,128)S(1)} %get-tuple-element.93) | copy-start | bytes 196612
  21.7 2.9 %copy-start.1 = (f32[256,16,64]{2,1,0:T(8,128)S(1)}, f32[256,16,64]{2,1,0:T(8,128)}, u32[]{:S(2)}) copy-start(f32[256,16,64]{2,1,0:T(8,128)} %copy.39) | copy-start | bytes 3145732
  21.7 3.5 %copy-start.2 = (f32[256,16,64]{2,1,0:T(8,128)S(1)}, f32[256,16,64]{2,1,0:T(8,128)}, u32[]{:S(2)}) copy-start(f32[256,16,64]{2,1,0:T(8,128)} %copy.40) | copy-start | bytes 3145732
  26.9 2.0 copy-start.7
  26.9 2.7 %copy-start.12 = (f32[16,16,16,64]{3,2,1,0:T(8,128)}, f32[16,16,16,64]{3,2,1,0:T(8,128)S(1)}, u32[]{:S(2)}) copy-start(f32[16,16,16,64]{3,2,1,0:T(8,128)S(1)} %get-tuple-element.36) | copy-start | bytes 3145732
  26.9 3.2 %copy-start.13 = (f32[16,16,16,64]{3,2,1,0:T(8,128)}, f32[16,16,16,64]{3,2,1,0:T(8,128)S(1)}, u32[]{:S(2)}) copy-start(f32[16,16,16,64]{3,2,1,0:T(8,128)S(1)} %get-tuple-element.37) | copy-start | bytes 3145732
  32.9 9.7 %copy-start.31 = (f32[3,16,64]{2,1,0:T(8,128)S(1)}, f32[3,16,64]{2,1,0:T(8,128)}, u32[]{:S(2)}) copy-start(f32[3,16,64]{2,1,0:T(8,128)} %get-tuple-element.48) | copy-start | bytes 36868
  32.9 10.6 %copy-start.30 = (f32[3,16,64]{2,1,0:T(8,128)S(1)}, f32[3,16,64]{2,1,0:T(8,128)}, u32[]{:S(2)}) copy-start(f32[3,16,64]{2,1,0:T(8,128)} %get-tuple-element.49) | copy-start | bytes 36868
  35.5 12.4 %copy-start.33 = (f32[1,16,64]{2,1,0:T(8,128)S(1)}, f32[1,16,64]{2,1,0:T(8,128)}, u32[]{:S(2)}) copy-start(f32[1,16,64]{2,1,0:T(8,128)} %get-tuple-element.101) | copy-start | bytes 12292
  39.6 9.4 %copy-start.32 = (f32[1,16,64]{2,1,0:T(8,128)S(1)}, f32[1,16,64]{2,1,0:T(8,128)}, u32[]{:S(2)}) copy-start(f32[1,16,64]{2,1,0:T(8,128)} %get-tuple-element.100) | copy-start | bytes 12292
  42.6 9.0 %copy-start.16 = (f32[8,16,64]{2,1,0:T(8,128)}, f32[8,16,64]{2,1,0:T(8,128)S(1)}, u32[]{:S(2)}) copy-start(f32[8,16,64]{2,1,0:T(8,128)S(1)} %add.451) | copy-start | bytes 98308
  44.9 10.1 %copy-start.17 = (f32[8,16,64]{2,1,0:T(8,128)}, f32[8,16,64]{2,1,0:T(8,128)S(1)}, u32[]{:S(2)}) copy-start(f32[8,16,64]{2,1,0:T(8,128)S(1)} %add.439) | copy-start | bytes 98308
  45.0 10.0 %copy-start.21 = (f32[16,16,64]{2,1,0:T(8,128)}, f32[16,16,64]{2,1,0:T(8,128)S(1)}, u32[]{:S(2)}) copy-start(f32[16,16,64]{2,1,0:T(8,128)S(1)} %pad.273) | copy-start | bytes 196612
  47.8 7.1 %copy-start.20 = (f32[16,16,64]{2,1,0:T(8,128)}, f32[16,16,64]{2,1,0:T(8,128)S(1)}, u32[]{:S(2)}) copy-start(f32[16,16,64]{2,1,0:T(8,128)S(1)} %pad.274) | copy-start | bytes 196612
  48.7 6.3 %copy-start.18 = (f32[8,16,64]{2,1,0:T(8,128)}, f32[8,16,64]{2,1,0:T(8,128)S(1)}, u32[]{:S(2)}) copy-start(f32[8,16,64]{2,1,0:T(8,128)S(1)} %pad_maximum_fusion.2) | copy-start | bytes 98308
  49.8 5.2 %copy-start.19 = (f32[8,16,64]{2,1,0:T(8,128)}, f32[8,16,64]{2,1,0:T(8,128)S(1)}, u32[]{:S(2)}) copy-start(f32[8,16,64]{2,1,0:T(8,128)S(1)} %pad_maximum_fusion.3) | copy-start | bytes 98308
  55.0 62.7 %all-to-all-start = ((f32[64,1,4096]{2,1,0:T(1,128)}), f32[64,1,4096]{2,1,0:T(1,128)S(1)}, u32[]{:S(2)}, u32[]{:S(2)}) async-start(f32[64,1,4096]{2,1,0:T(1,128)} %reshape.196), calls=%async_computation | async-start | bytes 2097152 | tf_op jit(solution)/shard_map/all_to_all | solution.py:16
  68.2 77.5 %all-gather.2.cloned.1.call-start = ((), (), s32[]{:S(2)}) async-start(), calls=%async_computation.4 | async-start | bytes 5242880 | tf_op jit(solution)/shard_map/all_gather | solution.py:196
  68.9 34.5 %copy-start.37 = (s32[64,2]{0,1:T(2,128)S(1)}, s32[64,2]{0,1:T(2,128)}, u32[]{:S(2)}) copy-start(s32[64,2]{0,1:T(2,128)} %param.34) | copy-start | bytes 1540
  127.8 2.3 copy-start.6
  127.8 2.2 copy-start.11
  134.3 11.4 %copy-start.26 = (bf16[64,2048]{1,0:T(8,128)(2,1)S(1)}, bf16[64,2048]{1,0:T(8,128)(2,1)}, u32[]{:S(2)}) copy-start(bf16[64,2048]{1,0:T(8,128)(2,1)} %param.32) | copy-start | bytes 786436
  134.3 11.4 %copy-start.36 = (f32[1024]{0:T(1024)S(1)}, f32[1024]{0:T(1024)}, u32[]{:S(2)}) copy-start(f32[1024]{0:T(1024)} %param.30) | copy-start | bytes 12292
  136.7 8.8 %all-to-all-start.1 = ((bf16[4,64,256]{2,1,0:T(8,128)(2,1)}), bf16[4,64,256]{2,1,0:T(8,128)(2,1)S(1)}, u32[]{:S(2)}, u32[]{:S(2)}) async-start(bf16[4,64,256]{2,1,0:T(8,128)(2,1)} %all_to_all.20), calls=%async_computation.1 | async-start | bytes 262144 | tf_op jit(solution)/shard_map/all_to_all | solution.py:190
  145.7 4.0 %copy-start.28 = (f32[2048]{0:T(1024)S(1)}, f32[2048]{0:T(1024)}, u32[]{:S(2)}) copy-start(f32[2048]{0:T(1024)} %param.33) | copy-start | bytes 24580
  193.5 3.5 %copy-start.15 = (bf16[256,2048]{1,0:T(8,128)(2,1)S(1)}, bf16[256,2048]{1,0:T(8,128)(2,1)}, u32[]{:S(2)}) copy-start(bf16[256,2048]{1,0:T(8,128)(2,1)} %reshape.160) | copy-start | bytes 3145732
  201.0 8.7 %copy-start.38 = (f32[64,2]{0,1:T(2,128)S(1)}, f32[64,2]{0,1:T(2,128)}, u32[]{:S(2)}) copy-start(f32[64,2]{0,1:T(2,128)} %param.35) | copy-start | bytes 1540
  203.2 34.5 %all-to-all-start.3 = ((bf16[64,4,2048]{2,1,0:T(4,128)(2,1)}), bf16[64,4,2048]{2,1,0:T(4,128)(2,1)}, u32[]{:S(2)}, u32[]{:S(2)}) async-start(bf16[64,4,2048]{2,1,0:T(4,128)(2,1)} %reshape.161), calls=%async_computation.3 | async-start | bytes 2097152 | tf_op jit(solution)/shard_map/all_to_all | solution.py:223
  240.9 5.5 %copy-start.4 = (f32[64,2048]{1,0:T(8,128)S(1)}, f32[64,2048]{1,0:T(8,128)}, u32[]{:S(2)}) copy-start(f32[64,2048]{1,0:T(8,128)} %copy-done.3) | copy-start | bytes 1572868
  243.6 3.4 %copy-start.35 = (f32[2048]{0:T(1024)S(1)}, f32[2048]{0:T(1024)}, u32[]{:S(2)}) copy-start(f32[2048]{0:T(1024)} %param.39) | copy-start | bytes 24580
  (13 other events, 17.4 us)
Sparse Core Ops, SparseCore 0:
  70.8 51.4 all-gather.1
where the time goes:
time: 259 us; the launch traced here: 255 us
  local copies, waits for them, and re-layouts  82.8 us (32%)
  other arithmetic  44.6 us (17%)
  blocking collectives  39.9 us (15%)
  waiting for transfers between devices  33.5 us (13%)
  starting transfers between devices  23.7 us (9%)
  matrix products  16 us (6%)
  between operations  14.4 us (6%)
    all_to_all x1, blocking collectives, local(): lax.all_to_all(outgoing, 'sp', split_axis=0, concat_axis=0, tiled=True)  39.9 us
    all_to_all x1, waiting for transfers between devices, local(): lax.all_to_all(produced.reshape(received.shape), 'sp', split_axis=0, conc...  28 us
    pad x22, local copies, waits for them, and re-layouts, local(): lax.associative_scan(chain_combine, (prefix_real[:, -1], prefix_imag[:, -...  19.1 us
    unnamed x91, local copies, waits for them, and re-layouts  19.1 us
    all_to_all x1, starting transfers between devices, copy_for_each(): return lax.all_to_all(copies, axis, split_axis=0, concat_axis=0, tiled=True)  13.2 us
    concatenate x12, other arithmetic, local(): lax.associative_scan(chain_combine, (prefix_real[:, -1], prefix_imag[:, -...  8.86 us
    add x16, other arithmetic, local(): lax.associative_scan(chain_combine, (prefix_real[:, -1], prefix_imag[:, -...  8.65 us
    all_to_all x1, starting transfers between devices, local(): lax.all_to_all(produced.reshape(received.shape), 'sp', split_axis=0, conc...  6.46 us
  transfers between devices with their start and end apart: 4, of which 2 were waited for; matrix products, arithmetic and copies ran while one was open for 24% of the time, Pallas kernels for 0%

commit v1 on v0

v1 whole, which is shorter than its diff:
```python
import jax
import jax.numpy as jnp
from jax import lax
from jax.experimental import pallas as pl
from jax.experimental.pallas import tpu as pltpu
from jax.sharding import PartitionSpec as P

PICKS = 2
MIX_WIDTH = 1024
MESH = pl.DeviceIdType.MESH

deep_alpha = 2.0**0.25

TOKENS = 256
GROUPS = 16
CHANNELS = 16
STATE = 64
WIDTH = 2048
ROWS = 64
PLANES = 8
PLANE = 8
TP = 4
PIECE = 64


def times(ar, ai, br, bi):
    return ar * br - ai * bi, ar * bi + ai * br


def layer_norm(values, scales):
    centered = values - jnp.mean(values, axis=-1, keepdims=True)
    variance = jnp.mean(centered * centered, axis=-1, keepdims=True)
    return centered * lax.rsqrt(variance + 1e-05) * scales


def pair_rows(ref):
    return jnp.concatenate(
        [ref[pl.ds(0, 8, stride=2), :], ref[pl.ds(1, 8, stride=2), :]], axis=1
    )


def remote(src, dst, send_sem, recv_sem, **where):
    return pltpu.make_async_remote_copy(
        src_ref=src,
        dst_ref=dst,
        send_sem=send_sem,
        recv_sem=recv_sem,
        device_id=where,
        device_id_type=MESH,
    )


def mixer_kernel(
    x_ref,
    ret_ref,
    real_ref,
    freq_ref,
    step_ref,
    in_real_ref,
    in_imag_ref,
    out_real_ref,
    out_imag_ref,
    skip_ref,
    gain_ref,
    proj_ref,
    residual_ref,
    mix_gain_ref,
    hidden_ref,
    drive_w,
    read_w,
    drive_re,
    drive_im,
    shrink,
    states,
    mine,
    plane_buf,
    plane_sum,
    column_buf,
    mixed,
    whole,
    gathered,
    param_buf,
    plane_send,
    plane_recv,
    column_send,
    column_recv,
    tp_send,
    tp_recv,
    own_sem,
    ring_send,
    ring_recv,
    twin_send,
    twin_recv,
):
    sp = lax.axis_index("sp")
    tp = lax.axis_index("tp")
    plane = lax.div(sp, PLANE)
    place = lax.rem(sp, PLANE)
    core = lax.rem(sp, 2)
    twin = sp + 1 - 2 * core
    right = lax.rem(tp + 1, TP)
    left = lax.rem(tp + TP - 1, TP)
    across = lax.rem(tp + 2, TP)

    barrier = pltpu.get_barrier_semaphore()

    def greet_plane(k, _):
        peer = plane * PLANE + lax.rem(place + k, PLANE)
        pl.semaphore_signal(barrier, inc=1, device_id={"sp": peer}, device_id_type=MESH)
        return 0

    def greet_column(k, _):
        peer = lax.rem(plane + k, PLANES) * PLANE + place
        pl.semaphore_signal(barrier, inc=1, device_id={"sp": peer}, device_id_type=MESH)
        return 0

    def greet_tp(k, _):
        pl.semaphore_signal(
            barrier, inc=1, device_id={"tp": lax.rem(tp + k, TP)}, device_id_type=MESH
        )
        return 0

    lax.fori_loop(1, TP, greet_tp, 0)
    lax.fori_loop(1, PLANE, greet_plane, 0)
    lax.fori_loop(1, PLANES, greet_column, 0)

    own_copy = pltpu.make_async_copy(proj_ref, gathered.at[tp], own_sem)
    own_copy.start()

    group_row = lax.broadcasted_iota(jnp.int32, (GROUPS, STATE), 0)
    log_step = jnp.zeros((GROUPS, STATE), jnp.float32)
    for g in range(GROUPS):
        log_step = jnp.where(group_row == g, step_ref[g], log_step)
    stride = jnp.exp(log_step)
    decay_real = real_ref[...]
    decay_freq = freq_ref[...]
    growth = decay_real * stride
    turning = decay_freq * stride
    grown = jnp.exp(growth)
    cosine = jnp.cos(turning)
    sine = jnp.sin(turning)
    half_sine = jnp.sin(0.5 * turning)
    expm1 = jnp.tanh(0.5 * growth) * (grown + 1.0)
    upper_real = expm1 * cosine - 2.0 * half_sine * half_sine
    upper_imag = grown * sine
    denominator = decay_real * decay_real + decay_freq * decay_freq
    factor_real = (upper_real * decay_real + upper_imag * decay_freq) / denominator
    factor_imag = (upper_imag * decay_real - upper_real * decay_freq) / denominator
    param_buf[0] = grown * cosine
    param_buf[1] = grown * sine
    keep_re = pair_rows(param_buf.at[0])
    keep_im = pair_rows(param_buf.at[1])

    nothing = jnp.zeros((CHANNELS, STATE), jnp.float32)
    drive_w[...] = jnp.zeros(drive_w.shape, jnp.bfloat16)
    for g in range(GROUPS):
        rows = pl.ds(g * CHANNELS, CHANNELS)
        b_re = jnp.transpose(in_real_ref[g])
        b_im = jnp.transpose(in_imag_ref[g])
        c_re = out_real_ref[g]
        c_im = out_imag_ref[g]
        f_re = factor_real[g : g + 1, :]
        f_im = factor_imag[g : g + 1, :]
        r_re = c_re * f_re - c_im * f_im
        r_im = -(c_re * f_im + c_im * f_re)
        if g % 2 == 0:
            b_row = [b_re, nothing, b_im, nothing]
            r_row = [r_re, nothing, r_im, nothing]
        else:
            b_row = [nothing, b_re, nothing, b_im]
            r_row = [nothing, r_re, nothing, r_im]
        b_row = jnp.concatenate(b_row, axis=1)
        drive_w[g // 2, rows, :] = b_row.astype(jnp.bfloat16)
        read_w[rows, :] = jnp.concatenate(r_row, axis=1).astype(jnp.bfloat16)

    kept = jnp.transpose(jnp.exp(ret_ref[...]))
    kept_hi = kept.astype(jnp.bfloat16)
    rest = kept - kept_hi.astype(jnp.float32)
    kept_mid = rest.astype(jnp.bfloat16)
    kept_lo = (rest - kept_mid.astype(jnp.float32)).astype(jnp.bfloat16)
    select_row = lax.broadcasted_iota(jnp.int32, (GROUPS, 8 * 128), 0)
    select_lane = lax.broadcasted_iota(jnp.int32, (GROUPS, 8 * 128), 1)
    select = (select_row == lax.div(select_lane, STATE)).astype(jnp.bfloat16)
    spread = (
        jnp.dot(kept_hi, select, preferred_element_type=jnp.float32)
        + jnp.dot(kept_mid, select, preferred_element_type=jnp.float32)
        + jnp.dot(kept_lo, select, preferred_element_type=jnp.float32)
    )
    x = x_ref[...]
    for j in range(8):
        at = pl.ds(j, TOKENS, stride=8)
        driven = jnp.dot(x, drive_w[j], preferred_element_type=jnp.float32)
        drive_re[at, :] = driven[:, :128]
        drive_im[at, :] = driven[:, 128:]
        shrink[at, :] = spread[:, j * 128 : (j + 1) * 128]

    pl.semaphore_wait(barrier, (TP - 1) + (PLANE - 1) + (PLANES - 1))

    half = core * (2 * PIECE)
    piece_lo = pl.ds(pl.multiple_of(half, PIECE), PIECE)
    piece_hi = pl.ds(pl.multiple_of(half + PIECE, PIECE), PIECE)

    def ring(block, piece, way, slot):
        to = right if way == 0 else left
        return remote(
            gathered.at[block, piece, :],
            gathered.at[block, piece, :],
            ring_send.at[slot],
            ring_recv.at[slot],
            tp=to,
        )

    own_copy.wait()
    to_right_lo = ring(tp, piece_lo, 0, 0)
    to_left_hi = ring(tp, piece_hi, 1, 1)
    to_right_hi = ring(tp, piece_hi, 0, 2)
    to_left_lo = ring(tp, piece_lo, 1, 3)
    to_right_lo.start()
    to_left_hi.start()
    to_right_hi.start()
    to_left_lo.start()

    def advance(t, carried):
        s_re, s_im, decay = carried
        row = pl.ds(pl.multiple_of(t * 8, 8), 8)
        shr = shrink[row, :]
        a_re = shr * keep_re
        a_im = shr * keep_im
        n_re = (a_re * s_re - a_im * s_im) + drive_re[row, :]
        n_im = (a_re * s_im + a_im * s_re) + drive_im[row, :]
        return n_re, n_im, decay * shr

    zero = jnp.zeros((8, 128), jnp.float32)
    one = jnp.ones((8, 128), jnp.float32)
    end_re, end_im, decay = lax.fori_loop(0, TOKENS, advance, (zero, zero, one), unroll=8)
    mine[0] = end_re
    mine[1] = end_im
    mine[2] = decay

    power_re, power_im = keep_re, keep_im
    for _ in range(8):
        power_re, power_im = times(power_re, power_im, power_re, power_im)
    plane_re, plane_im = power_re, power_im
    for _ in range(3):
        plane_re, plane_im = times(plane_re, plane_im, plane_re, plane_im)

    def plane_copy(k):
        peer = plane * PLANE + lax.rem(place + k, PLANE)
        return remote(mine, plane_buf.at[place], plane_send.at[k], plane_recv.at[place], sp=peer)

    def send_plane(k, _):
        plane_copy(k).start()
        return 0

    def plane_arrived(k, _):
        source = lax.rem(place + k, PLANE)
        remote(
            mine, plane_buf.at[source], plane_send.at[k], plane_recv.at[source], sp=plane * PLANE + source
        ).wait_recv()
        return 0

    lax.fori_loop(1, PLANE, send_plane, 0)
    lax.fori_loop(1, PLANE, plane_arrived, 0)
    plane_buf[place] = mine[...]

    def join(buf, k, carried, p_re, p_im):
        s_re, s_im, decay = carried
        d = buf[k, 2]
        m_re, m_im = times(d * p_re, d * p_im, s_re, s_im)
        return m_re + buf[k, 0], m_im + buf[k, 1], decay * d

    def join_place(k, carried):
        return join(plane_buf, k, carried, power_re, power_im)

    total = lax.fori_loop(0, PLANE, join_place, (zero, zero, one))
    plane_sum[0] = total[0]
    plane_sum[1] = total[1]
    plane_sum[2] = total[2]

    def column_copy(p):
        return remote(
            plane_sum, column_buf.at[plane], column_send.at[p], column_recv.at[plane], sp=p * PLANE + place
        )

    def send_column(p, _):
        column_copy(p).start()
        return 0

    def column_arrived(p, _):
        remote(
            plane_sum, column_buf.at[p], column_send.at[p], column_recv.at[p], sp=p * PLANE + place
        ).wait_recv()
        return 0

    lax.fori_loop(plane + 1, PLANES, send_column, 0)

    def twin_copy(block, piece, slot):
        return remote(
            gathered.at[block, piece, :],
            gathered.at[block, piece, :],
            twin_send.at[slot],
            twin_recv.at[slot],
            sp=twin,
        )

    from_left_lo = ring(left, piece_lo, 0, 0)
    from_right_hi = ring(right, piece_hi, 1, 1)
    from_left_hi = ring(left, piece_hi, 0, 2)
    from_right_lo = ring(right, piece_lo, 1, 3)
    from_left_lo.wait_recv()
    pass_right = ring(left, piece_lo, 0, 4)
    pass_right.start()
    from_right_hi.wait_recv()
    pass_left = ring(right, piece_hi, 1, 5)
    pass_left.start()
    twin_left_lo = twin_copy(left, piece_lo, 0)
    twin_right_hi = twin_copy(right, piece_hi, 1)
    twin_left_lo.start()
    twin_right_hi.start()

    lax.fori_loop(0, plane, column_arrived, 0)

    def join_plane(p, carried):
        return join(column_buf, p, carried, plane_re, plane_im)

    carried = lax.fori_loop(0, plane, join_plane, (zero, zero, one))
    carried = lax.fori_loop(0, place, join_place, carried)

    def record(t, carried):
        s_re, s_im = carried
        row = pl.ds(pl.multiple_of(t * 8, 8), 8)
        shr = shrink[row, :]
        a_re = shr * keep_re
        a_im = shr * keep_im
        n_re = (a_re * s_re - a_im * s_im) + drive_re[row, :]
        n_im = (a_re * s_im + a_im * s_re) + drive_im[row, :]
        states[row, :128] = n_re
        states[row, 128:] = n_im
        return n_re, n_im

    lax.fori_loop(0, TOKENS, record, (carried[0], carried[1]), unroll=8)

    def read(k, _):
        at = pl.ds(pl.multiple_of(k * 256, 256), 256)
        product = lax.dot_general(
            states[at, :].astype(jnp.bfloat16),
            read_w[...],
            (((1,), (1,)), ((), ())),
            preferred_element_type=jnp.float32,
        )
        drive_re[at, :] = product[:, :128]
        drive_im[at, :] = product[:, 128:]
        return 0

    lax.fori_loop(0, 8, read, 0)
    lane = lax.broadcasted_iota(jnp.int32, (TOKENS, 128), 1)
    for side, buf in ((0, drive_re), (1, drive_im)):
        picked = jnp.zeros((TOKENS, 128), jnp.float32)
        for j in range(4):
            value = buf[pl.ds(side * 4 + j, TOKENS, stride=8), :]
            picked = jnp.where(lax.div(lane, 32) == j, value, picked)
        skip = jnp.concatenate([skip_ref[g : g + 1, :] for g in range(side * 8, side * 8 + 8)], axis=1)
        lanes = slice(side * 128, side * 128 + 128)
        read_out = picked + skip * x_ref[:, lanes].astype(jnp.float32)
        mixed[:, lanes] = jax.nn.gelu(read_out).astype(jnp.bfloat16)

    def tp_copy(k):
        peer = lax.rem(tp + k, TP)
        rows = pl.ds(pl.multiple_of(peer * ROWS, ROWS), ROWS)
        return remote(mixed.at[rows, :], whole.at[tp], tp_send.at[k], tp_recv.at[tp], tp=peer)

    def send_tp(k, _):
        tp_copy(k).start()
        return 0

    def tp_arrived(k, _):
        source = lax.rem(tp + k, TP)
        rows = pl.ds(pl.multiple_of(tp * ROWS, ROWS), ROWS)
        remote(mixed.at[rows, :], whole.at[source], tp_send.at[k], tp_recv.at[source], tp=source).wait_recv()
        return 0

    lax.fori_loop(1, TP, send_tp, 0)
    whole[tp] = mixed[pl.ds(pl.multiple_of(tp * ROWS, ROWS), ROWS), :]

    from_left_hi.wait_recv()
    from_right_lo.wait_recv()
    twin_left_hi = twin_copy(left, piece_hi, 2)
    twin_right_lo = twin_copy(right, piece_lo, 3)
    twin_left_hi.start()
    twin_right_lo.start()
    across_lo = ring(across, piece_lo, 0, 4)
    across_hi = ring(across, piece_hi, 1, 5)
    across_lo.wait_recv()
    twin_across_lo = twin_copy(across, piece_lo, 4)
    twin_across_lo.start()
    across_hi.wait_recv()
    twin_across_hi = twin_copy(across, piece_hi, 5)
    twin_across_hi.start()

    other = 2 * PIECE - half
    other_lo = pl.ds(pl.multiple_of(other, PIECE), PIECE)
    other_hi = pl.ds(pl.multiple_of(other + PIECE, PIECE), PIECE)
    lax.fori_loop(1, TP, tp_arrived, 0)
    for slot, (block, piece) in enumerate(
        (
            (left, other_lo),
            (right, other_hi),
            (left, other_hi),
            (right, other_lo),
            (across, other_lo),
            (across, other_hi),
        )
    ):
        twin_copy(block, piece, slot).wait_recv()

    squares = jnp.zeros((ROWS, 1), jnp.float32)
    scaled = []
    for q in range(TP):
        rows = whole[q].astype(jnp.float32)
        squares += jnp.sum(rows * rows, axis=1, keepdims=True)
        scaled.append((rows * gain_ref[:, q * 256 : (q + 1) * 256]).astype(jnp.bfloat16))
    inverse = lax.rsqrt(squares / MIX_WIDTH + 1e-06)
    mix = jnp.zeros((ROWS, WIDTH), jnp.float32)
    for q in range(TP):
        mix += jnp.dot(scaled[q], gathered[q], preferred_element_type=jnp.float32)
    mix = deep_alpha * residual_ref[...].astype(jnp.float32) + mix * inverse
    hidden_ref[...] = layer_norm(mix, mix_gain_ref[...]).astype(jnp.bfloat16)

    def plane_left(k, _):
        plane_copy(k).wait_send()
        return 0

    def column_left(p, _):
        column_copy(p).wait_send()
        return 0

    def tp_left(k, _):
        tp_copy(k).wait_send()
        return 0

    lax.fori_loop(1, PLANE, plane_left, 0)
    lax.fori_loop(plane + 1, PLANES, column_left, 0)
    lax.fori_loop(1, TP, tp_left, 0)
    for copy in (to_right_lo, to_left_hi, to_right_hi, to_left_lo, pass_right, pass_left):
        copy.wait_send()
    for copy in (twin_left_lo, twin_right_hi, twin_left_hi, twin_right_lo, twin_across_lo, twin_across_hi):
        copy.wait_send()


def mixer(
    mixer_input,
    retention,
    decay_real,
    decay_freq,
    log_step,
    input_real,
    input_imag,
    readout_real,
    readout_imaginary,
    skip_weight,
    norm_gain,
    projection,
    residual,
    mix_gain,
):
    vmem = pl.BlockSpec(memory_space=pltpu.VMEM)
    smem = pl.BlockSpec(memory_space=pltpu.SMEM)
    hbm = pl.BlockSpec(memory_space=pltpu.HBM)
    f32 = jnp.float32
    bf16 = jnp.bfloat16
    dma = pltpu.SemaphoreType.DMA
    return pl.pallas_call(
        mixer_kernel,
        out_shape=jax.ShapeDtypeStruct((ROWS, WIDTH), bf16),
        in_specs=[vmem, vmem, vmem, vmem, smem, vmem, vmem, vmem, vmem, vmem, vmem, hbm, vmem, vmem],
        out_specs=vmem,
        scratch_shapes=[
            pltpu.VMEM((8, 256, 256), bf16),
            pltpu.VMEM((256, 256), bf16),
            pltpu.VMEM((TOKENS * 8, 128), f32),
            pltpu.VMEM((TOKENS * 8, 128), f32),
            pltpu.VMEM((TOKENS * 8, 128), f32),
            pltpu.VMEM((TOKENS * 8, 256), f32),
            pltpu.VMEM((3, 8, 128), f32),
            pltpu.VMEM((PLANE, 3, 8, 128), f32),
            pltpu.VMEM((3, 8, 128), f32),
            pltpu.VMEM((PLANES, 3, 8, 128), f32),
            pltpu.VMEM((TOKENS, 256), bf16),
            pltpu.VMEM((TP, ROWS, 256), bf16),
            pltpu.VMEM((TP, 256, WIDTH), bf16),
            pltpu.VMEM((2, GROUPS, STATE), f32),
            dma((PLANE,)),
            dma((PLANE,)),
            dma((PLANES,)),
            dma((PLANES,)),
            dma((TP,)),
            dma((TP,)),
            dma(()),
            dma((6,)),
            dma((6,)),
            dma((6,)),
            dma((6,)),
        ],
        compiler_params=pltpu.CompilerParams(
            collective_id=0, has_side_effects=True, vmem_limit_bytes=40 * 1024 * 1024
        ),
        name="mixer",
    )(
        mixer_input,
        retention,
        decay_real,
        decay_freq,
        log_step,
        input_real,
        input_imag,
        readout_real,
        readout_imaginary,
        skip_weight,
        norm_gain.reshape(1, -1),
        projection,
        residual,
        mix_gain.reshape(1, -1),
    )


def local(
    mixer_input,
    retention,
    decay_real,
    decay_freq,
    log_step,
    input_real,
    input_imag,
    readout_real,
    readout_imaginary,
    skip_weight,
    norm_gain,
    projection,
    residual,
    mix_gain,
    routes,
    route_weight,
    expert_gate,
    expert_up,
    expert_down,
    final_gain,
):
    hidden = mixer(
        mixer_input,
        retention,
        decay_real,
        decay_freq,
        log_step,
        input_real,
        input_imag,
        readout_real,
        readout_imaginary,
        skip_weight,
        norm_gain,
        projection,
        residual,
        mix_gain,
    )
    row_count = hidden.shape[0]
    expert_count = lax.axis_size("sp")
    capacity = max(2, 2 * row_count * PICKS // expert_count)
    chosen = routes.reshape(-1)
    onehot = (chosen[:, None] == jnp.arange(expert_count, dtype=jnp.int32)[None, :]).astype(
        jnp.int32
    )
    slot_index = jnp.sum((jnp.cumsum(onehot, axis=0) - 1) * onehot, axis=1)
    target = chosen * capacity + slot_index
    source_row = jnp.full((expert_count * capacity,), row_count, jnp.int32)
    source_row = source_row.at[target].set(jnp.arange(row_count * PICKS, dtype=jnp.int32) // PICKS)
    padded = jnp.concatenate([hidden, jnp.zeros((1, hidden.shape[1]), hidden.dtype)], axis=0)
    outgoing = padded[source_row].reshape(expert_count, capacity, -1)
    received = lax.all_to_all(outgoing, "sp", split_axis=0, concat_axis=0, tiled=True)
    arrived = received.reshape(-1, received.shape[2])
    gate_act = jnp.dot(arrived, expert_gate[0], preferred_element_type=jnp.float32)
    up_act = jnp.dot(arrived, expert_up[0], preferred_element_type=jnp.float32)
    active = (jax.nn.silu(gate_act) * up_act).astype(jnp.bfloat16)
    produced = jnp.dot(active, expert_down[0], preferred_element_type=jnp.float32).astype(
        jnp.bfloat16
    )
    returned = lax.all_to_all(
        produced.reshape(received.shape), "sp", split_axis=0, concat_axis=0, tiled=True
    )
    gathered_rows = returned.reshape(expert_count * capacity, -1)[target].reshape(
        row_count, PICKS, -1
    )
    expert_mix = jnp.sum(route_weight[:, :, None] * gathered_rows.astype(jnp.float32), axis=1)
    layer_out = layer_norm(deep_alpha * hidden.astype(jnp.float32) + expert_mix, final_gain)
    return layer_out.astype(jnp.bfloat16)


def solution(mesh):
    in_specs = (
        P("sp", "tp"),
        P("tp", "sp"),
        P("tp", None),
        P("tp", None),
        P("tp"),
        P("tp", None, None),
        P("tp", None, None),
        P("tp", None, None),
        P("tp", None, None),
        P("tp", None),
        P(),
        P("tp", None),
        P(("sp", "tp"), None),
        P(),
        P(("sp", "tp"), None),
        P(("sp", "tp"), None),
        P("sp", None, None),
        P("sp", None, None),
        P("sp", None, None),
        P(),
    )
    out_specs = P(("sp", "tp"), None)
    return jax.shard_map(local, mesh=mesh, in_specs=in_specs, out_specs=out_specs, check_vma=False)
```

time: 259 us -> 141 us (0.54); the launches traced: 255 us -> 140 us
  local copies, waits for them, and re-layouts: 82.8 us -> 26.5 us
  other arithmetic: 44.6 us -> 3.95 us
  Pallas kernels: 0 us -> 33.4 us
  starting transfers between devices: 23.7 us -> 6.48 us
  between operations: 14.4 us -> 0.17 us
  matrix products: 16 us -> 7.12 us
  waiting for transfers between devices: 33.5 us -> 28 us
  blocking collectives: 39.9 us -> 34.6 us
    pallas_call x0 -> x1, Pallas kernels: none -> 33.4 us  [mixer(): pl.pallas_call(mixer_kernel, out_shape=jax.ShapeDtypeStruct((ROWS, WIDTH)...]
    pad x22 -> x0, local copies, waits for them, and re-layouts: 19.1 us -> none  [local(): lax.associative_scan(chain_combine, (prefix_real[:, -1], prefix_imag[:, -...]
    all_to_all x2 -> x0, starting transfers between devices: 17.2 us -> none  [the longest x1 13.2 us: copy_for_each(): return lax.all_to_all(copies, axis, split_axis=0, concat_axis=0, tiled=True)]
    slice x11 -> x0, local copies, waits for them, and re-layouts: 14.4 us -> none  [the longest x9 5.11 us: local(): lax.associative_scan(chain_combine, (prefix_real[:, -1], prefix_imag[:, -...]
    add x28 -> x0, other arithmetic: 12.6 us -> none  [the longest x16 8.65 us: local(): lax.associative_scan(chain_combine, (prefix_real[:, -1], prefix_imag[:, -...]
    concatenate x13 -> x0, other arithmetic: 8.87 us -> none  [the longest x12 8.86 us: local(): lax.associative_scan(chain_combine, (prefix_real[:, -1], prefix_imag[:, -...]
    dot_general x5 -> x0, matrix products: 8.54 us -> none  [the longest x1 3.16 us: local(): jnp.dot(scaled, lax.all_gather(projection, 'tp', axis=0, tiled=True), pre...]
    transpose x2 -> x0, local copies, waits for them, and re-layouts: 6.22 us -> none  [the longest x1 3.73 us: local(): drive_real = jnp.einsum('tgc,gpc->tgp', inputs, bar_real)]
  transfers between devices with their start and end apart: 4 -> 1, of which waited for: 2 -> 1; matrix products, arithmetic and copies ran while one was open for 24% -> 0% of each run, Pallas kernels for 0% -> 0%
where the time goes in v1:
time: 141 us; the launch traced here: 140 us
  blocking collectives  34.6 us (25%)
  Pallas kernels  33.4 us (24%)
  waiting for transfers between devices  28 us (20%)
  local copies, waits for them, and re-layouts  26.5 us (19%)
  matrix products  7.12 us (5%)
  starting transfers between devices  6.48 us (5%)
  other arithmetic  3.95 us (3%)
    all_to_all x1, blocking collectives, local(): lax.all_to_all(outgoing, 'sp', split_axis=0, concat_axis=0, tiled=True)  34.6 us
    pallas_call x1, Pallas kernels, mixer(): pl.pallas_call(mixer_kernel, out_shape=jax.ShapeDtypeStruct((ROWS, WIDTH)...  33.4 us
    all_to_all x1, waiting for transfers between devices, local(): lax.all_to_all(produced.reshape(received.shape), 'sp', split_axis=0, conc...  28 us
    unnamed x34, local copies, waits for them, and re-layouts  13 us
    all_to_all x1, starting transfers between devices, local(): lax.all_to_all(produced.reshape(received.shape), 'sp', split_axis=0, conc...  6.48 us
    dot_general x1, matrix products, local(): jnp.dot(active, expert_down[0], preferred_element_type=jnp.float32)  4 us
    dot_general x1, matrix products, local(): jnp.dot(arrived, expert_gate[0], preferred_element_type=jnp.float32)  3.11 us
  transfers between devices with their start and end apart: 1, of which 1 were waited for; matrix products, arithmetic and copies ran while one was open for 0% of the time, Pallas kernels for 0%

profile of v1, /device:TPU:1, one launch (start us, length us, event | category | flops | bytes accessed | tf_op | source)
XLA Modules:
  0.0 140.1 jit_solution(4694370648154699756)
XLA Ops:
  0.0 0.9 copy.30
  0.9 0.7 broadcast_multiply_fusion
  1.6 1.1 copy.26.in_real_ref
  2.7 1.1 copy.27.in_imag_ref
  4.7 1.0 scatter_custom_fusion
  5.7 1.2 copy-done.1
  6.9 0.9 copy-done.2
  7.9 0.9 copy-done.3
  8.8 0.9 copy-done.4
  9.7 0.9 copy-done.5
  10.6 0.7 copy-done.6
  11.3 0.7 copy-done.7
  12.0 0.7 copy-done.8
  12.7 0.7 copy-done.9
  13.4 0.7 copy-done.10
  14.1 0.7 copy-done.11
  14.8 0.7 copy-done.12
  15.4 33.4 %mixer.1 = bf16[64,2048]{1,0:T(8,128)(2,1)S(1)} custom-call(bf16[256,256]{1,0:T(8,128)(2,1)S(1)} %copy-done.3, f32[16,256]{1,0:T(8,128)S(1)} %copy-done.6, f32[16,64]{1,0:T(8,128)S(1)} %copy-done.7, f32[16,64]{1,0:T(8,128)S(1)} %copy-done.8, f32[16]{0:T(128)S(1)} %copy-done.12, f32[16,64,16]{2,1,0:T(8,128)S(1)} %copy.26.in_real_ref, ...), custom_call_target="tpu_custom_call" | custom-call | tf_op jit(solution)/shard_map/mixer/pallas_call | solution.py:472
  48.8 2.3 %gather_fusion = bf16[256,2048]{1,0:T(8,128)(2,1)} fusion(bf16[65,2048]{1,0:T(8,128)(2,1)S(1)} %concatenate.3, s32[1024]{0:T(1024)S(1)} %pad_clamp_fusion.1), kind=kCustom, calls=%fused_computation | custom fusion | bytes 2098176 | tf_op jit(solution)/shard_map/gather | solution.py:576
  51.2 1.5 %reshape.67 = bf16[64,4,2048]{2,1,0:T(4,128)(2,1)S(1)} reshape(bf16[256,2048]{1,0:T(8,128)(2,1)} %gather_fusion) | data formatting | bytes 2097152 | tf_op jit(solution)/shard_map/reshape | solution.py:576
  52.6 34.6 %all_to_all.10 = bf16[64,4,2048]{2,1,0:T(4,128)(2,1)} all-to-all(bf16[64,4,2048]{2,1,0:T(4,128)(2,1)S(1)} %reshape.67), channel_id=1, replica_groups=mesh['sp'=64,'tp'=4] {'sp'}, dimensions={0} | all-to-all | bytes 2097152 | tf_op jit(solution)/shard_map/all_to_all | solution.py:577
  87.2 1.3 reshape.68
  88.5 3.1 %fusion.3 = f32[256,512]{1,0:T(8,128)} fusion(bf16[256,2048]{1,0:T(8,128)(2,1)S(1)} %reshape.68, bf16[1,2048,512]{2,1,0:T(8,128)(2,1)} %param.36), kind=kOutput, calls=%fused_computation.7 | convolution fusion | flops 536870912 | bytes 3670016 | tf_op jit(solution)/shard_map/dot_general | solution.py:579
  91.7 4.0 %convolution_convert_fusion = bf16[256,2048]{1,0:T(8,128)(2,1)} fusion(bf16[1,512,2048]{2,1,0:T(8,128)(2,1)S(1)} %copy-done, bf16[256,2048]{1,0:T(8,128)(2,1)S(1)} %reshape.68, bf16[1,2048,512]{2,1,0:T(8,128)(2,1)} %param.37, f32[256,512]{1,0:T(8,128)} %fusion.3), kind=kOutput, calls=%fused_computation.3 | convolution fusion | flops 1075052544 | bytes 6815744 | tf_op jit(solution)/shard_map/dot_general | solution.py:582
  95.7 2.3 %reshape.69 = bf16[64,4,2048]{2,1,0:T(4,128)(2,1)} reshape(bf16[256,2048]{1,0:T(8,128)(2,1)} %convolution_convert_fusion) | data formatting | bytes 2097152 | tf_op jit(solution)/shard_map/reshape | solution.py:586
  97.9 6.5 %all-to-all-start.1 = ((bf16[64,4,2048]{2,1,0:T(4,128)(2,1)}), bf16[64,4,2048]{2,1,0:T(4,128)(2,1)}, u32[]{:S(2)}, u32[]{:S(2)}) async-start(bf16[64,4,2048]{2,1,0:T(4,128)(2,1)} %reshape.69), calls=%async_computation.1 | async-start | bytes 2097152 | tf_op jit(solution)/shard_map/all_to_all | solution.py:585
  104.5 28.0 %all-to-all-done.1 = bf16[64,4,2048]{2,1,0:T(4,128)(2,1)} async-done(((bf16[64,4,2048]{2,1,0:T(4,128)(2,1)}), bf16[64,4,2048]{2,1,0:T(4,128)(2,1)}, u32[]{:S(2)}, u32[]{:S(2)}) %all-to-all-start.1) | async-done | bytes 1048608 | tf_op jit(solution)/shard_map/all_to_all | solution.py:585
  132.5 1.3 reshape.70
  133.8 1.7 %gather_fusion.1 = bf16[128,2048]{1,0:T(8,128)(2,1)} fusion(bf16[256,2048]{1,0:T(8,128)(2,1)S(1)} %reshape.70, s32[1024]{0:T(1024)S(1)} %pad_clamp_fusion), kind=kCustom, calls=%fused_computation.1 | custom fusion | bytes 1049088 | tf_op jit(solution)/shard_map/gather | solution.py:588
  135.6 1.7 %reshape.71 = f32[64,2,2048]{2,1,0:T(2,128)S(1)} reshape(bf16[128,2048]{1,0:T(8,128)(2,1)} %gather_fusion.1) | data formatting | bytes 1572864 | tf_op jit(solution)/shard_map/convert_element_type | solution.py:591
  137.3 1.5 %multiply_reduce_fusion = f32[64,2048]{1,0:T(8,128)S(1)} fusion(f32[64,2,2048]{2,1,0:T(2,128)S(1)} %reshape.71, f32[64,2]{1,0:T(8,128)S(1)} %copy.28), kind=kLoop, calls=%fused_computation.11 | loop fusion | flops 393216 | bytes 1573376 | tf_op jit(solution)/shard_map/reduce_sum | solution.py:591
  139.3 0.9 multiply_convert_fusion
  (35 shorter events, 1.4 us)
Async XLA Ops:
  0.0 91.7 %copy-start = (bf16[1,512,2048]{2,1,0:T(8,128)(2,1)S(1)}, bf16[1,512,2048]{2,1,0:T(8,128)(2,1)}, u32[]{:S(2)}) copy-start(bf16[1,512,2048]{2,1,0:T(8,128)(2,1)} %param.38) | copy-start | bytes 6291460
  5.7 1.2 copy-start.1
  6.9 0.9 copy-start.2
  7.9 0.9 copy-start.3
  8.8 0.9 copy-start.4
  9.7 0.9 copy-start.5
  10.6 0.7 copy-start.6
  11.3 0.7 copy-start.7
  12.0 0.7 copy-start.8
  12.7 0.7 copy-start.9
  13.4 0.7 copy-start.10
  14.1 0.7 copy-start.11
  14.8 0.7 copy-start.12
  95.7 8.8 %copy-start.14 = (f32[64,2]{0,1:T(2,128)S(1)}, f32[64,2]{0,1:T(2,128)}, u32[]{:S(2)}) copy-start(f32[64,2]{0,1:T(2,128)} %param.35) | copy-start | bytes 1540
  97.9 34.6 %all-to-all-start.1 = ((bf16[64,4,2048]{2,1,0:T(4,128)(2,1)}), bf16[64,4,2048]{2,1,0:T(4,128)(2,1)}, u32[]{:S(2)}, u32[]{:S(2)}) async-start(bf16[64,4,2048]{2,1,0:T(4,128)(2,1)} %reshape.69), calls=%async_computation.1 | async-start | bytes 2097152 | tf_op jit(solution)/shard_map/all_to_all | solution.py:585
  135.6 3.7 %copy-start.13 = (f32[2048]{0:T(1024)S(1)}, f32[2048]{0:T(1024)}, u32[]{:S(2)}) copy-start(f32[2048]{0:T(1024)} %param.39) | copy-start | bytes 24580

commit v2 on v1

--- a/solution.py
+++ b/solution.py
@@ -21,6 +21,10 @@
 PLANE = 8
 TP = 4
 PIECE = 64
+EXPERTS = 64
+CAPACITY = 4
+SLOTS = EXPERTS * CAPACITY
+HIDDEN = 512
 
 
 def times(ar, ai, br, bi):
@@ -50,22 +54,46 @@
     )
 
 
-def mixer_kernel(
+def layer_kernel(
+    step_ref,
+    x_hbm,
+    ret_hbm,
+    real_hbm,
+    freq_hbm,
+    in_real_hbm,
+    in_imag_hbm,
+    out_real_hbm,
+    out_imag_hbm,
+    skip_hbm,
+    gain_hbm,
+    residual_hbm,
+    mix_gain_hbm,
+    routes_hbm,
+    weight_hbm,
+    final_gain_hbm,
+    proj_ref,
+    gate_hbm,
+    up_hbm,
+    down_hbm,
+    layer_ref,
     x_ref,
     ret_ref,
     real_ref,
     freq_ref,
-    step_ref,
     in_real_ref,
     in_imag_ref,
     out_real_ref,
     out_imag_ref,
     skip_ref,
     gain_ref,
-    proj_ref,
     residual_ref,
     mix_gain_ref,
-    hidden_ref,
+    routes_ref,
+    weight_ref,
+    final_gain_ref,
+    gate,
+    up,
+    down,
     drive_w,
     read_w,
     drive_re,
@@ -80,6 +108,13 @@
     whole,
     gathered,
     param_buf,
+    hidden_buf,
+    combine_hi,
+    outgoing,
+    arrived,
+    produced,
+    returned,
+    load_sem,
     plane_send,
     plane_recv,
     column_send,
@@ -91,6 +126,10 @@
     ring_recv,
     twin_send,
     twin_recv,
+    out_send,
+    out_recv,
+    back_send,
+    back_recv,
 ):
     sp = lax.axis_index("sp")
     tp = lax.axis_index("tp")
@@ -126,6 +165,35 @@
 
     own_copy = pltpu.make_async_copy(proj_ref, gathered.at[tp], own_sem)
     own_copy.start()
+    loads = [
+        pltpu.make_async_copy(source, target, load_sem.at[k])
+        for k, (source, target) in enumerate(
+            (
+                (real_hbm, real_ref),
+                (freq_hbm, freq_ref),
+                (in_real_hbm, in_real_ref),
+                (in_imag_hbm, in_imag_ref),
+                (out_real_hbm, out_real_ref),
+                (out_imag_hbm, out_imag_ref),
+                (ret_hbm, ret_ref),
+                (x_hbm, x_ref),
+                (skip_hbm, skip_ref),
+                (routes_hbm, routes_ref),
+                (weight_hbm, weight_ref),
+                (gain_hbm, gain_ref),
+                (mix_gain_hbm, mix_gain_ref),
+                (final_gain_hbm, final_gain_ref),
+                (residual_hbm, residual_ref),
+                (gate_hbm.at[0], gate),
+                (up_hbm.at[0], up),
+                (down_hbm.at[0], down),
+            )
+        )
+    ]
+    for load in loads:
+        load.start()
+    for load in loads[:8]:
+        load.wait()
 
     group_row = lax.broadcasted_iota(jnp.int32, (GROUPS, STATE), 0)
     log_step = jnp.zeros((GROUPS, STATE), jnp.float32)
@@ -294,6 +362,26 @@
 
     lax.fori_loop(plane + 1, PLANES, send_column, 0)
 
+    for load in loads[8:15]:
+        load.wait()
+    slot = lax.broadcasted_iota(jnp.int32, (ROWS, SLOTS), 1)
+    slot_plane = lax.rem(plane + lax.shift_right_logical(slot, 5), PLANES)
+    slot_place = lax.rem(place + lax.rem(lax.shift_right_logical(slot, 2), PLANE), PLANE)
+    slot_expert = slot_plane * PLANE + slot_place
+    first = jnp.where(routes_ref[:, 0:1] == slot_expert, 1.0, 0.0)
+    second = jnp.where(routes_ref[:, 1:2] == slot_expert, 1.0, 0.0)
+    named = first + second
+    row_at = lax.broadcasted_iota(jnp.int32, (ROWS, ROWS), 0)
+    row_before = lax.broadcasted_iota(jnp.int32, (ROWS, ROWS), 1)
+    earlier = jnp.where(row_before < row_at, 1.0, 0.0).astype(jnp.bfloat16)
+    rank = jnp.dot(earlier, named.astype(jnp.bfloat16), preferred_element_type=jnp.float32)
+    here = jnp.where(rank == lax.rem(slot, CAPACITY).astype(jnp.float32), 1.0, 0.0)
+    weights = here * (weight_ref[:, 0:1] * first + weight_ref[:, 1:2] * second)
+    weights_hi = weights.astype(jnp.bfloat16)
+    combine_hi[:ROWS, :] = weights_hi
+    combine_hi[ROWS:, :] = (weights - weights_hi.astype(jnp.float32)).astype(jnp.bfloat16)
+    pick = jnp.transpose(here * named).astype(jnp.bfloat16)
+
     def twin_copy(block, piece, slot):
         return remote(
             gathered.at[block, piece, :],
@@ -424,7 +512,89 @@
     for q in range(TP):
         mix += jnp.dot(scaled[q], gathered[q], preferred_element_type=jnp.float32)
     mix = deep_alpha * residual_ref[...].astype(jnp.float32) + mix * inverse
-    hidden_ref[...] = layer_norm(mix, mix_gain_ref[...]).astype(jnp.bfloat16)
+    hidden = layer_norm(mix, mix_gain_ref[...]).astype(jnp.bfloat16)
+    hidden_buf[...] = hidden
+
+    def expert_of(k):
+        return lax.rem(plane + lax.div(k, PLANE), PLANES) * PLANE + lax.rem(place + k, PLANE)
+
+    def source_of(k):
+        return lax.rem(plane + PLANES - lax.div(k, PLANE), PLANES) * PLANE + lax.rem(
+            place + PLANE - lax.rem(k, PLANE), PLANE
+        )
+
+    def out_copy(k):
+        return remote(outgoing.at[k], arrived.at[k], out_send.at[k], out_recv.at[k], sp=expert_of(k))
+
+    def back_copy(k):
+        return remote(produced.at[k], returned.at[k], back_send.at[k], back_recv.at[k], sp=source_of(k))
+
+    def send_out(k, _):
+        out_copy(k).start()
+        return 0
+
+    for p in (4, 3, 5, 2, 6, 1, 7, 0):
+        rows = jnp.dot(pick[p * 32 : (p + 1) * 32, :], hidden, preferred_element_type=jnp.float32)
+        outgoing[p * PLANE : (p + 1) * PLANE] = rows.astype(jnp.bfloat16).reshape(PLANE, CAPACITY, WIDTH)
+        lax.fori_loop(p * PLANE + (p == 0), (p + 1) * PLANE, send_out, 0)
+    arrived[0] = outgoing[0]
+
+    for load in loads[15:]:
+        load.wait()
+
+    def expert(c, _):
+        far = (PLANES // 2 + c) * PLANE
+        near = (PLANES // 2 - 1 - c) * PLANE
+        near_first = jnp.maximum(near, 1)
+
+        def out_arrived(k, _):
+            out_copy(k).wait_recv()
+            return 0
+
+        def send_back(k, _):
+            back_copy(k).start()
+            return 0
+
+        lax.fori_loop(far, far + PLANE, out_arrived, 0)
+        lax.fori_loop(near_first, near + PLANE, out_arrived, 0)
+        rows = jnp.concatenate(
+            [
+                arrived[pl.ds(far, PLANE)].reshape(PLANE * CAPACITY, WIDTH),
+                arrived[pl.ds(near, PLANE)].reshape(PLANE * CAPACITY, WIDTH),
+            ],
+            axis=0,
+        )
+        gate_act = jnp.dot(rows, gate[...], preferred_element_type=jnp.float32)
+        up_act = jnp.dot(rows, up[...], preferred_element_type=jnp.float32)
+        active = (jax.nn.silu(gate_act) * up_act).astype(jnp.bfloat16)
+        result = jnp.dot(active, down[...], preferred_element_type=jnp.float32).astype(jnp.bfloat16)
+        produced[pl.ds(far, PLANE)] = result[: PLANE * CAPACITY].reshape(PLANE, CAPACITY, WIDTH)
+        produced[pl.ds(near, PLANE)] = result[PLANE * CAPACITY :].reshape(PLANE, CAPACITY, WIDTH)
+        lax.fori_loop(far, far + PLANE, send_back, 0)
+        lax.fori_loop(near_first, near + PLANE, send_back, 0)
+        return 0
+
+    lax.fori_loop(0, PLANES // 2, expert, 0)
+    returned[0] = produced[0]
+
+    def back_arrived(k, _):
+        back_copy(k).wait_recv()
+        return 0
+
+    lax.fori_loop(1, EXPERTS, back_arrived, 0)
+    both = jnp.dot(
+        combine_hi[...], returned[...].reshape(SLOTS, WIDTH), preferred_element_type=jnp.float32
+    )
+    expert_mix = both[:ROWS] + both[ROWS:]
+    final = layer_norm(deep_alpha * hidden_buf[...].astype(jnp.float32) + expert_mix, final_gain_ref[...])
+    layer_ref[...] = final.astype(jnp.bfloat16)
+
+    def out_left(k, _):
+        out_copy(k).wait_send()
+        back_copy(k).wait_send()
+        return 0
+
+    lax.fori_loop(1, EXPERTS, out_left, 0)
 
     def plane_left(k, _):
         plane_copy(k).wait_send()
@@ -445,82 +615,6 @@
         copy.wait_send()
     for copy in (twin_left_lo, twin_right_hi, twin_left_hi, twin_right_lo, twin_across_lo, twin_across_hi):
         copy.wait_send()
-
-
-def mixer(
-    mixer_input,
-    retention,
-    decay_real,
-    decay_freq,
-    log_step,
-    input_real,
-    input_imag,
-    readout_real,
-    readout_imaginary,
-    skip_weight,
-    norm_gain,
-    projection,
-    residual,
-    mix_gain,
-):
-    vmem = pl.BlockSpec(memory_space=pltpu.VMEM)
-    smem = pl.BlockSpec(memory_space=pltpu.SMEM)
-    hbm = pl.BlockSpec(memory_space=pltpu.HBM)
-    f32 = jnp.float32
-    bf16 = jnp.bfloat16
-    dma = pltpu.SemaphoreType.DMA
-    return pl.pallas_call(
-        mixer_kernel,
-        out_shape=jax.ShapeDtypeStruct((ROWS, WIDTH), bf16),
-        in_specs=[vmem, vmem, vmem, vmem, smem, vmem, vmem, vmem, vmem, vmem, vmem, hbm, vmem, vmem],
-        out_specs=vmem,
-        scratch_shapes=[
-            pltpu.VMEM((8, 256, 256), bf16),
-            pltpu.VMEM((256, 256), bf16),
-            pltpu.VMEM((TOKENS * 8, 128), f32),
-            pltpu.VMEM((TOKENS * 8, 128), f32),
-            pltpu.VMEM((TOKENS * 8, 128), f32),
-            pltpu.VMEM((TOKENS * 8, 256), f32),
-            pltpu.VMEM((3, 8, 128), f32),
-            pltpu.VMEM((PLANE, 3, 8, 128), f32),
-            pltpu.VMEM((3, 8, 128), f32),
-            pltpu.VMEM((PLANES, 3, 8, 128), f32),
-            pltpu.VMEM((TOKENS, 256), bf16),
-            pltpu.VMEM((TP, ROWS, 256), bf16),
-            pltpu.VMEM((TP, 256, WIDTH), bf16),
-            pltpu.VMEM((2, GROUPS, STATE), f32),
-            dma((PLANE,)),
-            dma((PLANE,)),
-            dma((PLANES,)),
-            dma((PLANES,)),
-            dma((TP,)),
-            dma((TP,)),
-            dma(()),
-            dma((6,)),
-            dma((6,)),
-            dma((6,)),
-            dma((6,)),
-        ],
-        compiler_params=pltpu.CompilerParams(
-            collective_id=0, has_side_effects=True, vmem_limit_bytes=40 * 1024 * 1024
-        ),
-        name="mixer",
-    )(
-        mixer_input,
-        retention,
-        decay_real,
-        decay_freq,
-        log_step,
-        input_real,
-        input_imag,
-        readout_real,
-        readout_imaginary,
-        skip_weight,
-        norm_gain.reshape(1, -1),
-        projection,
-        residual,
-        mix_gain.reshape(1, -1),
-    )
 
 
 def local(
@@ -545,52 +639,82 @@
     expert_down,
     final_gain,
 ):
-    hidden = mixer(
+    hbm = pl.BlockSpec(memory_space=pltpu.HBM)
+    smem = pl.BlockSpec(memory_space=pltpu.SMEM)
+    vmem = pl.BlockSpec(memory_space=pltpu.VMEM)
+    f32 = jnp.float32
+    bf16 = jnp.bfloat16
+    dma = pltpu.SemaphoreType.DMA
+    small = (
         mixer_input,
         retention,
         decay_real,
         decay_freq,
-        log_step,
         input_real,
         input_imag,
         readout_real,
         readout_imaginary,
         skip_weight,
-        norm_gain,
-        projection,
+        norm_gain.reshape(1, -1),
         residual,
-        mix_gain,
+        mix_gain.reshape(1, -1),
+        routes,
+        route_weight,
+        final_gain.reshape(1, -1),
     )
-    row_count = hidden.shape[0]
-    expert_count = lax.axis_size("sp")
-    capacity = max(2, 2 * row_count * PICKS // expert_count)
-    chosen = routes.reshape(-1)
-    onehot = (chosen[:, None] == jnp.arange(expert_count, dtype=jnp.int32)[None, :]).astype(
-        jnp.int32
-    )
-    slot_index = jnp.sum((jnp.cumsum(onehot, axis=0) - 1) * onehot, axis=1)
-    target = chosen * capacity + slot_index
-    source_row = jnp.full((expert_count * capacity,), row_count, jnp.int32)
-    source_row = source_row.at[target].set(jnp.arange(row_count * PICKS, dtype=jnp.int32) // PICKS)
-    padded = jnp.concatenate([hidden, jnp.zeros((1, hidden.shape[1]), hidden.dtype)], axis=0)
-    outgoing = padded[source_row].reshape(expert_count, capacity, -1)
-    received = lax.all_to_all(outgoing, "sp", split_axis=0, concat_axis=0, tiled=True)
-    arrived = received.reshape(-1, received.shape[2])
-    gate_act = jnp.dot(arrived, expert_gate[0], preferred_element_type=jnp.float32)
-    up_act = jnp.dot(arrived, expert_up[0], preferred_element_type=jnp.float32)
-    active = (jax.nn.silu(gate_act) * up_act).astype(jnp.bfloat16)
-    produced = jnp.dot(active, expert_down[0], preferred_element_type=jnp.float32).astype(
-        jnp.bfloat16
-    )
-    returned = lax.all_to_all(
-        produced.reshape(received.shape), "sp", split_axis=0, concat_axis=0, tiled=True
-    )
-    gathered_rows = returned.reshape(expert_count * capacity, -1)[target].reshape(
-        row_count, PICKS, -1
-    )
-    expert_mix = jnp.sum(route_weight[:, :, None] * gathered_rows.astype(jnp.float32), axis=1)
-    layer_out = layer_norm(deep_alpha * hidden.astype(jnp.float32) + expert_mix, final_gain)
-    return layer_out.astype(jnp.bfloat16)
+    large = (projection, expert_gate, expert_up, expert_down)
+    return pl.pallas_call(
+        layer_kernel,
+        out_shape=jax.ShapeDtypeStruct((ROWS, WIDTH), bf16),
+        in_specs=[smem] + [hbm] * (len(small) + len(large)),
+        out_specs=vmem,
+        scratch_shapes=[pltpu.VMEM(a.shape, a.dtype) for a in small]
+        + [
+            pltpu.VMEM((WIDTH, HIDDEN), bf16),
+            pltpu.VMEM((WIDTH, HIDDEN), bf16),
+            pltpu.VMEM((HIDDEN, WIDTH), bf16),
+            pltpu.VMEM((8, 256, 256), bf16),
+            pltpu.VMEM((256, 256), bf16),
+            pltpu.VMEM((TOKENS * 8, 128), f32),
+            pltpu.VMEM((TOKENS * 8, 128), f32),
+            pltpu.VMEM((TOKENS * 8, 128), f32),
+            pltpu.VMEM((TOKENS * 8, 256), f32),
+            pltpu.VMEM((3, 8, 128), f32),
+            pltpu.VMEM((PLANE, 3, 8, 128), f32),
+            pltpu.VMEM((3, 8, 128), f32),
+            pltpu.VMEM((PLANES, 3, 8, 128), f32),
+            pltpu.VMEM((TOKENS, 256), bf16),
+            pltpu.VMEM((TP, ROWS, 256), bf16),
+            pltpu.VMEM((TP, 256, WIDTH), bf16),
+            pltpu.VMEM((2, GROUPS, STATE), f32),
+            pltpu.VMEM((ROWS, WIDTH), bf16),
+            pltpu.VMEM((2 * ROWS, SLOTS), bf16),
+            pltpu.VMEM((EXPERTS, CAPACITY, WIDTH), bf16),
+            pltpu.VMEM((EXPERTS, CAPACITY, WIDTH), bf16),
+            pltpu.VMEM((EXPERTS, CAPACITY, WIDTH), bf16),
+            pltpu.VMEM((EXPERTS, CAPACITY, WIDTH), bf16),
+            dma((18,)),
+            dma((PLANE,)),
+            dma((PLANE,)),
+            dma((PLANES,)),
+            dma((PLANES,)),
+            dma((TP,)),
+            dma((TP,)),
+            dma(()),
+            dma((6,)),
+            dma((6,)),
+            dma((6,)),
+            dma((6,)),
+            dma((EXPERTS,)),
+            dma((EXPERTS,)),
+            dma((EXPERTS,)),
+            dma((EXPERTS,)),
+        ],
+        compiler_params=pltpu.CompilerParams(
+            collective_id=0, has_side_effects=True, vmem_limit_bytes=56 * 1024 * 1024
+        ),
+        name="layer",
+    )(log_step, *small, *large)
 
 
 def solution(mesh):

time: 141 us -> 96.6 us (0.69)
  Pallas kernels: 33.4 us -> 88.2 us
  blocking collectives: 34.6 us -> 0 us
  waiting for transfers between devices: 28 us -> 0 us
  local copies, waits for them, and re-layouts: 26.5 us -> 8.25 us
  matrix products: 7.12 us -> 0 us
  starting transfers between devices: 6.48 us -> 0 us
  other arithmetic: 3.95 us -> 0 us
    pallas_call x1, Pallas kernels: 33.4 us -> 88.2 us  [local(): pl.pallas_call(layer_kernel, out_shape=jax.ShapeDtypeStruct((ROWS, WIDTH)...]
    all_to_all x1 -> x0, blocking collectives: 34.6 us -> none  [local(): lax.all_to_all(outgoing, 'sp', split_axis=0, concat_axis=0, tiled=True)]
    all_to_all x1 -> x0, waiting for transfers between devices: 28 us -> none  [local(): lax.all_to_all(produced.reshape(received.shape), 'sp', split_axis=0, conc...]
    dot_general x2 -> x0, matrix products: 7.12 us -> none  [the longest x1 4 us: local(): jnp.dot(active, expert_down[0], preferred_element_type=jnp.float32)]
    all_to_all x1 -> x0, starting transfers between devices: 6.48 us -> none  [local(): lax.all_to_all(produced.reshape(received.shape), 'sp', split_axis=0, conc...]
    reshape x4 -> x0, local copies, waits for them, and re-layouts: 6.4 us -> none  [the longest x1 2.28 us: local(): produced.reshape(received.shape)]
    unnamed x34 -> x5, local copies, waits for them, and re-layouts: 13 us -> 8.25 us
    gather x2 -> x0, local copies, waits for them, and re-layouts: 4.06 us -> none  [the longest x1 2.35 us: local(): outgoing = padded[source_row].reshape(expert_count, capacity, -1)]
  transfers between devices with their start and end apart: 1 -> 0, of which waited for: 1 -> 0; matrix products, arithmetic and copies ran while one was open for 0% -> 0% of each run, Pallas kernels for 0% -> 0%
where the time goes in v2:
time: 96.6 us; the launch traced here: 96.4 us
  Pallas kernels  88.2 us (91%)
  local copies, waits for them, and re-layouts  8.25 us (9%)
    pallas_call x1, Pallas kernels, local(): pl.pallas_call(layer_kernel, out_shape=jax.ShapeDtypeStruct((ROWS, WIDTH)...  88.2 us
    unnamed x5, local copies, waits for them, and re-layouts  8.25 us

profile of v2, /device:TPU:1, one launch (start us, length us, event | category | flops | bytes accessed | tf_op | source)
XLA Modules:
  0.0 96.4 jit_solution(9863530469843878214)
XLA Ops:
  0.0 1.4 %copy.23.routes_hbm = s32[64,2]{1,0:T(8,128)} copy(s32[64,2]{0,1:T(2,128)} %param.34) | data formatting | bytes 1024 | tf_op args[14]
  1.4 1.4 %copy.24.weight_hbm = f32[64,2]{1,0:T(8,128)} copy(f32[64,2]{0,1:T(2,128)} %param.35) | data formatting | bytes 1024 | tf_op args[15]
  2.7 1.9 %copy.21.in_real_hbm = f32[16,64,16]{2,1,0:T(8,128)} copy(f32[16,64,16]{1,2,0:T(8,128)} %param.25) | data formatting | bytes 131072 | tf_op args[5]
  4.7 1.9 %copy.22.in_imag_hbm = f32[16,64,16]{2,1,0:T(8,128)} copy(f32[16,64,16]{1,2,0:T(8,128)} %param.26) | data formatting | bytes 131072 | tf_op args[6]
  6.6 88.2 %layer.1 = bf16[64,2048]{1,0:T(8,128)(2,1)} custom-call(f32[16]{0:T(128)} %step_ref.1, bf16[256,256]{1,0:T(8,128)(2,1)} %x_hbm.1, f32[16,256]{1,0:T(8,128)} %ret_hbm.1, f32[16,64]{1,0:T(8,128)} %real_hbm.1, f32[16,64]{1,0:T(8,128)} %freq_hbm.1, f32[16,64,16]{2,1,0:T(8,128)} %copy.21.in_real_hbm, f32[16,64,16]{2,1,0:T(8,128)} %copy.22.in_imag_hbm, ...), custom_call_target="tpu_custom_call" | custom-call | tf_op jit(solution)/shard_map/layer/pallas_call | solution.py:666
  94.7 1.7 %copy.26 = bf16[64,2048]{1,0:T(8,128)(2,1)} copy(bf16[64,2048]{1,0:T(8,128)(2,1)} %layer.1) | data formatting | bytes 524288

commit v3 on v2

--- a/solution.py
+++ b/solution.py
@@ -25,6 +25,8 @@
 CAPACITY = 4
 SLOTS = EXPERTS * CAPACITY
 HIDDEN = 512
+FAR = 16
+FAR_BLOCKS = 32
 
 
 def times(ar, ai, br, bi):
@@ -110,6 +112,9 @@
     param_buf,
     hidden_buf,
     combine_hi,
+    pick,
+    mixed_out,
+    mixed_in,
     outgoing,
     arrived,
     produced,
@@ -130,6 +135,8 @@
     out_recv,
     back_send,
     back_recv,
+    mixed_send,
+    mixed_recv,
 ):
     sp = lax.axis_index("sp")
     tp = lax.axis_index("tp")
@@ -223,8 +230,8 @@
     drive_w[...] = jnp.zeros(drive_w.shape, jnp.bfloat16)
     for g in range(GROUPS):
         rows = pl.ds(g * CHANNELS, CHANNELS)
-        b_re = jnp.transpose(in_real_ref[g])
-        b_im = jnp.transpose(in_imag_ref[g])
+        b_re = in_real_ref[g]
+        b_im = in_imag_ref[g]
         c_re = out_real_ref[g]
         c_im = out_imag_ref[g]
         f_re = factor_real[g : g + 1, :]
@@ -364,23 +371,58 @@
 
     for load in loads[8:15]:
         load.wait()
-    slot = lax.broadcasted_iota(jnp.int32, (ROWS, SLOTS), 1)
+    slot = lax.broadcasted_iota(jnp.int32, (SLOTS, ROWS), 0)
     slot_plane = lax.rem(plane + lax.shift_right_logical(slot, 5), PLANES)
     slot_place = lax.rem(place + lax.rem(lax.shift_right_logical(slot, 2), PLANE), PLANE)
     slot_expert = slot_plane * PLANE + slot_place
-    first = jnp.where(routes_ref[:, 0:1] == slot_expert, 1.0, 0.0)
-    second = jnp.where(routes_ref[:, 1:2] == slot_expert, 1.0, 0.0)
+    first = jnp.where(routes_ref[0:1, :] == slot_expert, 1.0, 0.0)
+    second = jnp.where(routes_ref[1:2, :] == slot_expert, 1.0, 0.0)
     named = first + second
-    row_at = lax.broadcasted_iota(jnp.int32, (ROWS, ROWS), 0)
-    row_before = lax.broadcasted_iota(jnp.int32, (ROWS, ROWS), 1)
+    row_before = lax.broadcasted_iota(jnp.int32, (ROWS, ROWS), 0)
+    row_at = lax.broadcasted_iota(jnp.int32, (ROWS, ROWS), 1)
     earlier = jnp.where(row_before < row_at, 1.0, 0.0).astype(jnp.bfloat16)
-    rank = jnp.dot(earlier, named.astype(jnp.bfloat16), preferred_element_type=jnp.float32)
+    rank = jnp.dot(named.astype(jnp.bfloat16), earlier, preferred_element_type=jnp.float32)
     here = jnp.where(rank == lax.rem(slot, CAPACITY).astype(jnp.float32), 1.0, 0.0)
-    weights = here * (weight_ref[:, 0:1] * first + weight_ref[:, 1:2] * second)
+    weights = jnp.transpose(here * (weight_ref[0:1, :] * first + weight_ref[1:2, :] * second))
     weights_hi = weights.astype(jnp.bfloat16)
     combine_hi[:ROWS, :] = weights_hi
     combine_hi[ROWS:, :] = (weights - weights_hi.astype(jnp.float32)).astype(jnp.bfloat16)
-    pick = jnp.transpose(here * named).astype(jnp.bfloat16)
+    pick[...] = (here * named).astype(jnp.bfloat16)
+
+    def expert_of(k):
+        return lax.rem(plane + lax.div(k, PLANE), PLANES) * PLANE + lax.rem(place + k, PLANE)
+
+    def source_of(k):
+        return lax.rem(plane + PLANES - lax.div(k, PLANE), PLANES) * PLANE + lax.rem(
+            place + PLANE - lax.rem(k, PLANE), PLANE
+        )
+
+    def out_copy(k):
+        return remote(outgoing.at[k], arrived.at[k], out_send.at[k], out_recv.at[k], sp=expert_of(k))
+
+    def mixed_copy(k):
+        return remote(
+            mixed_out.at[k], mixed_in.at[k], mixed_send.at[k], mixed_recv.at[k], sp=expert_of(k + FAR)
+        )
+
+    def back_copy(k):
+        return remote(produced.at[k], returned.at[k], back_send.at[k], back_recv.at[k], sp=source_of(k))
+
+    def send_out(k, _):
+        out_copy(k).start()
+        return 0
+
+    def send_mixed(k, _):
+        mixed_copy(k).start()
+        return 0
+
+    def blocks(p, rows):
+        picked = jnp.dot(pick[p * 32 : (p + 1) * 32, :], rows, preferred_element_type=jnp.float32)
+        return picked.astype(jnp.bfloat16).reshape(PLANE, CAPACITY, rows.shape[1])
+
+    for p in (4, 3, 5, 2):
+        outgoing[p * PLANE : (p + 1) * PLANE] = blocks(p, residual_ref[...])
+        lax.fori_loop(p * PLANE, (p + 1) * PLANE, send_out, 0)
 
     def twin_copy(block, piece, slot):
         return remote(
@@ -489,6 +531,26 @@
     other_lo = pl.ds(pl.multiple_of(other, PIECE), PIECE)
     other_hi = pl.ds(pl.multiple_of(other + PIECE, PIECE), PIECE)
     lax.fori_loop(1, TP, tp_arrived, 0)
+
+    for p in (4, 3, 5, 2):
+        q = p - FAR // PLANE
+        for piece in range(TP):
+            lanes = slice(piece * 256, (piece + 1) * 256)
+            mixed_out[q * PLANE : (q + 1) * PLANE, :, lanes] = blocks(p, whole[piece])
+        lax.fori_loop(q * PLANE, (q + 1) * PLANE, send_mixed, 0)
+
+    def hidden_of(pieces, residual_rows):
+        squares = jnp.zeros((ROWS, 1), jnp.float32)
+        mix = jnp.zeros((ROWS, WIDTH), jnp.float32)
+        for q in range(TP):
+            rows = pieces[q].astype(jnp.float32)
+            squares += jnp.sum(rows * rows, axis=1, keepdims=True)
+            scaled = (rows * gain_ref[:, q * 256 : (q + 1) * 256]).astype(jnp.bfloat16)
+            mix += jnp.dot(scaled, gathered[q], preferred_element_type=jnp.float32)
+        inverse = lax.rsqrt(squares / MIX_WIDTH + 1e-06)
+        mix = deep_alpha * residual_rows.astype(jnp.float32) + mix * inverse
+        return layer_norm(mix, mix_gain_ref[...]).astype(jnp.bfloat16)
+
     for slot, (block, piece) in enumerate(
         (
             (left, other_lo),
@@ -500,49 +562,23 @@
         )
     ):
         twin_copy(block, piece, slot).wait_recv()
-
-    squares = jnp.zeros((ROWS, 1), jnp.float32)
-    scaled = []
-    for q in range(TP):
-        rows = whole[q].astype(jnp.float32)
-        squares += jnp.sum(rows * rows, axis=1, keepdims=True)
-        scaled.append((rows * gain_ref[:, q * 256 : (q + 1) * 256]).astype(jnp.bfloat16))
-    inverse = lax.rsqrt(squares / MIX_WIDTH + 1e-06)
-    mix = jnp.zeros((ROWS, WIDTH), jnp.float32)
-    for q in range(TP):
-        mix += jnp.dot(scaled[q], gathered[q], preferred_element_type=jnp.float32)
-    mix = deep_alpha * residual_ref[...].astype(jnp.float32) + mix * inverse
-    hidden = layer_norm(mix, mix_gain_ref[...]).astype(jnp.bfloat16)
-    hidden_buf[...] = hidden
-
-    def expert_of(k):
-        return lax.rem(plane + lax.div(k, PLANE), PLANES) * PLANE + lax.rem(place + k, PLANE)
-
-    def source_of(k):
-        return lax.rem(plane + PLANES - lax.div(k, PLANE), PLANES) * PLANE + lax.rem(
-            place + PLANE - lax.rem(k, PLANE), PLANE
-        )
-
-    def out_copy(k):
-        return remote(outgoing.at[k], arrived.at[k], out_send.at[k], out_recv.at[k], sp=expert_of(k))
-
-    def back_copy(k):
-        return remote(produced.at[k], returned.at[k], back_send.at[k], back_recv.at[k], sp=source_of(k))
-
-    def send_out(k, _):
-        out_copy(k).start()
-        return 0
-
-    for p in (4, 3, 5, 2, 6, 1, 7, 0):
-        rows = jnp.dot(pick[p * 32 : (p + 1) * 32, :], hidden, preferred_element_type=jnp.float32)
-        outgoing[p * PLANE : (p + 1) * PLANE] = rows.astype(jnp.bfloat16).reshape(PLANE, CAPACITY, WIDTH)
+    hidden_buf[...] = hidden_of([whole[q] for q in range(TP)], residual_ref[...])
+
+    for p in (6, 1, 7, 0):
+        outgoing[p * PLANE : (p + 1) * PLANE] = blocks(p, hidden_buf[...])
         lax.fori_loop(p * PLANE + (p == 0), (p + 1) * PLANE, send_out, 0)
     arrived[0] = outgoing[0]
 
     for load in loads[15:]:
         load.wait()
 
-    def expert(c, _):
+    def rows_of(buf, far, near):
+        size = PLANE * CAPACITY
+        return jnp.concatenate(
+            [buf[pl.ds(far, PLANE)].reshape(size, -1), buf[pl.ds(near, PLANE)].reshape(size, -1)], axis=0
+        )
+
+    def expert(c, is_far):
         far = (PLANES // 2 + c) * PLANE
         near = (PLANES // 2 - 1 - c) * PLANE
         near_first = jnp.maximum(near, 1)
@@ -551,19 +587,22 @@
             out_copy(k).wait_recv()
             return 0
 
+        def mixed_arrived(k, _):
+            mixed_copy(k).wait_recv()
+            return 0
+
         def send_back(k, _):
             back_copy(k).start()
             return 0
 
         lax.fori_loop(far, far + PLANE, out_arrived, 0)
         lax.fori_loop(near_first, near + PLANE, out_arrived, 0)
-        rows = jnp.concatenate(
-            [
-                arrived[pl.ds(far, PLANE)].reshape(PLANE * CAPACITY, WIDTH),
-                arrived[pl.ds(near, PLANE)].reshape(PLANE * CAPACITY, WIDTH),
-            ],
-            axis=0,
-        )
+        rows = rows_of(arrived, far, near)
+        if is_far:
+            lax.fori_loop(far - FAR, far - FAR + PLANE, mixed_arrived, 0)
+            lax.fori_loop(near - FAR, near - FAR + PLANE, mixed_arrived, 0)
+            mixed_rows = rows_of(mixed_in, far - FAR, near - FAR)
+            rows = hidden_of([mixed_rows[:, q * 256 : (q + 1) * 256] for q in range(TP)], rows)
         gate_act = jnp.dot(rows, gate[...], preferred_element_type=jnp.float32)
         up_act = jnp.dot(rows, up[...], preferred_element_type=jnp.float32)
         active = (jax.nn.silu(gate_act) * up_act).astype(jnp.bfloat16)
@@ -572,9 +611,17 @@
         produced[pl.ds(near, PLANE)] = result[PLANE * CAPACITY :].reshape(PLANE, CAPACITY, WIDTH)
         lax.fori_loop(far, far + PLANE, send_back, 0)
         lax.fori_loop(near_first, near + PLANE, send_back, 0)
-        return 0
-
-    lax.fori_loop(0, PLANES // 2, expert, 0)
+
+    def far_expert(c, _):
+        expert(c, True)
+        return 0
+
+    def near_expert(c, _):
+        expert(c, False)
+        return 0
+
+    lax.fori_loop(0, 2, far_expert, 0)
+    lax.fori_loop(2, 4, near_expert, 0)
     returned[0] = produced[0]
 
     def back_arrived(k, _):
@@ -594,7 +641,12 @@
         back_copy(k).wait_send()
         return 0
 
+    def mixed_left(k, _):
+        mixed_copy(k).wait_send()
+        return 0
+
     lax.fori_loop(1, EXPERTS, out_left, 0)
+    lax.fori_loop(0, FAR_BLOCKS, mixed_left, 0)
 
     def plane_left(k, _):
         plane_copy(k).wait_send()
@@ -650,16 +702,16 @@
         retention,
         decay_real,
         decay_freq,
-        input_real,
-        input_imag,
+        jnp.transpose(input_real, (0, 2, 1)),
+        jnp.transpose(input_imag, (0, 2, 1)),
         readout_real,
         readout_imaginary,
         skip_weight,
         norm_gain.reshape(1, -1),
         residual,
         mix_gain.reshape(1, -1),
-        routes,
-        route_weight,
+        jnp.transpose(routes),
+        jnp.transpose(route_weight),
         final_gain.reshape(1, -1),
     )
     large = (projection, expert_gate, expert_up, expert_down)
@@ -689,6 +741,9 @@
             pltpu.VMEM((2, GROUPS, STATE), f32),
             pltpu.VMEM((ROWS, WIDTH), bf16),
             pltpu.VMEM((2 * ROWS, SLOTS), bf16),
+            pltpu.VMEM((SLOTS, ROWS), bf16),
+            pltpu.VMEM((FAR_BLOCKS, CAPACITY, MIX_WIDTH), bf16),
+            pltpu.VMEM((FAR_BLOCKS, CAPACITY, MIX_WIDTH), bf16),
             pltpu.VMEM((EXPERTS, CAPACITY, WIDTH), bf16),
             pltpu.VMEM((EXPERTS, CAPACITY, WIDTH), bf16),
             pltpu.VMEM((EXPERTS, CAPACITY, WIDTH), bf16),
@@ -709,9 +764,11 @@
             dma((EXPERTS,)),
             dma((EXPERTS,)),
             dma((EXPERTS,)),
+            dma((FAR_BLOCKS,)),
+            dma((FAR_BLOCKS,)),
         ],
         compiler_params=pltpu.CompilerParams(
-            collective_id=0, has_side_effects=True, vmem_limit_bytes=56 * 1024 * 1024
+            collective_id=0, has_side_effects=True, vmem_limit_bytes=62 * 1024 * 1024
         ),
         name="layer",
     )(log_step, *small, *large)

time: 96.6 us -> 85.1 us (0.88)
  local copies, waits for them, and re-layouts: 8.25 us -> 1.67 us
  Pallas kernels: 88.2 us -> 83.3 us
    unnamed x5 -> x1, local copies, waits for them, and re-layouts: 8.25 us -> 1.67 us
    pallas_call x1, Pallas kernels: 88.2 us -> 83.3 us  [local(): pl.pallas_call(layer_kernel, out_shape=jax.ShapeDtypeStruct((ROWS, WIDTH)...]
where the time goes in v3:
time: 85.1 us; the launch traced here: 85 us
  Pallas kernels  83.3 us (98%)
  local copies, waits for them, and re-layouts  1.67 us (2%)
    pallas_call x1, Pallas kernels, local(): pl.pallas_call(layer_kernel, out_shape=jax.ShapeDtypeStruct((ROWS, WIDTH)...  83.3 us

profile of v3, /device:TPU:1, one launch (start us, length us, event | category | flops | bytes accessed | tf_op | source)
XLA Modules:
  0.0 85.0 jit_solution(1672103378814899974)
XLA Ops:
  0.0 83.3 %layer.1 = bf16[64,2048]{1,0:T(8,128)(2,1)} custom-call(f32[16]{0:T(128)} %step_ref.1, bf16[256,256]{1,0:T(8,128)(2,1)} %x_hbm.1, f32[16,256]{1,0:T(8,128)} %ret_hbm.1, f32[16,64]{1,0:T(8,128)} %real_hbm.1, f32[16,64]{1,0:T(8,128)} %freq_hbm.1, f32[16,16,64]{2,1,0:T(8,128)} %bitcast.7, f32[16,16,64]{2,1,0:T(8,128)} %bitcast.8, f32[16,16,64]{2,1,0:T(8,128)} %out_real_hbm.1, ...), custom_call_target="tpu_custom_call" | custom-call | tf_op jit(solution)/shard_map/layer/pallas_call | solution.py:718
  83.3 1.7 %copy.22 = bf16[64,2048]{1,0:T(8,128)(2,1)} copy(bf16[64,2048]{1,0:T(8,128)(2,1)} %layer.1) | data formatting | bytes 524288

commit v4 on v3

--- a/solution.py
+++ b/solution.py
@@ -25,8 +25,6 @@
 CAPACITY = 4
 SLOTS = EXPERTS * CAPACITY
 HIDDEN = 512
-FAR = 16
-FAR_BLOCKS = 32
 
 
 def times(ar, ai, br, bi):
@@ -335,39 +333,6 @@
         return 0
 
     lax.fori_loop(1, PLANE, send_plane, 0)
-    lax.fori_loop(1, PLANE, plane_arrived, 0)
-    plane_buf[place] = mine[...]
-
-    def join(buf, k, carried, p_re, p_im):
-        s_re, s_im, decay = carried
-        d = buf[k, 2]
-        m_re, m_im = times(d * p_re, d * p_im, s_re, s_im)
-        return m_re + buf[k, 0], m_im + buf[k, 1], decay * d
-
-    def join_place(k, carried):
-        return join(plane_buf, k, carried, power_re, power_im)
-
-    total = lax.fori_loop(0, PLANE, join_place, (zero, zero, one))
-    plane_sum[0] = total[0]
-    plane_sum[1] = total[1]
-    plane_sum[2] = total[2]
-
-    def column_copy(p):
-        return remote(
-            plane_sum, column_buf.at[plane], column_send.at[p], column_recv.at[plane], sp=p * PLANE + place
-        )
-
-    def send_column(p, _):
-        column_copy(p).start()
-        return 0
-
-    def column_arrived(p, _):
-        remote(
-            plane_sum, column_buf.at[p], column_send.at[p], column_recv.at[p], sp=p * PLANE + place
-        ).wait_recv()
-        return 0
-
-    lax.fori_loop(plane + 1, PLANES, send_column, 0)
 
     for load in loads[8:15]:
         load.wait()
@@ -402,7 +367,7 @@
 
     def mixed_copy(k):
         return remote(
-            mixed_out.at[k], mixed_in.at[k], mixed_send.at[k], mixed_recv.at[k], sp=expert_of(k + FAR)
+            mixed_out.at[k], mixed_in.at[k], mixed_send.at[k], mixed_recv.at[k], sp=expert_of(k)
         )
 
     def back_copy(k):
@@ -420,9 +385,112 @@
         picked = jnp.dot(pick[p * 32 : (p + 1) * 32, :], rows, preferred_element_type=jnp.float32)
         return picked.astype(jnp.bfloat16).reshape(PLANE, CAPACITY, rows.shape[1])
 
-    for p in (4, 3, 5, 2):
+    for p in (2, 6, 3, 5):
         outgoing[p * PLANE : (p + 1) * PLANE] = blocks(p, residual_ref[...])
+
+    lax.fori_loop(1, PLANE, plane_arrived, 0)
+    plane_buf[place] = mine[...]
+
+    def join(buf, k, carried, p_re, p_im):
+        s_re, s_im, decay = carried
+        d = buf[k, 2]
+        m_re, m_im = times(d * p_re, d * p_im, s_re, s_im)
+        return m_re + buf[k, 0], m_im + buf[k, 1], decay * d
+
+    def join_place(k, carried):
+        return join(plane_buf, k, carried, power_re, power_im)
+
+    total = lax.fori_loop(0, PLANE, join_place, (zero, zero, one))
+    plane_sum[0] = total[0]
+    plane_sum[1] = total[1]
+    plane_sum[2] = total[2]
+
+    def column_copy(p):
+        return remote(
+            plane_sum, column_buf.at[plane], column_send.at[p], column_recv.at[plane], sp=p * PLANE + place
+        )
+
+    def send_column(p, _):
+        column_copy(p).start()
+        return 0
+
+    def column_arrived(p, _):
+        remote(
+            plane_sum, column_buf.at[p], column_send.at[p], column_recv.at[p], sp=p * PLANE + place
+        ).wait_recv()
+        return 0
+
+    lax.fori_loop(plane + 1, PLANES, send_column, 0)
+
+    for p in (2, 6):
         lax.fori_loop(p * PLANE, (p + 1) * PLANE, send_out, 0)
+
+    lax.fori_loop(0, plane, column_arrived, 0)
+
+    for p in (3, 5):
+        lax.fori_loop(p * PLANE, (p + 1) * PLANE, send_out, 0)
+
+    def join_plane(p, carried):
+        return join(column_buf, p, carried, plane_re, plane_im)
+
+    carried = lax.fori_loop(0, plane, join_plane, (zero, zero, one))
+    carried = lax.fori_loop(0, place, join_place, carried)
+
+    def record(t, carried):
+        s_re, s_im = carried
+        row = pl.ds(pl.multiple_of(t * 8, 8), 8)
+        shr = shrink[row, :]
+        a_re = shr * keep_re
+        a_im = shr * keep_im
+        n_re = (a_re * s_re - a_im * s_im) + drive_re[row, :]
+        n_im = (a_re * s_im + a_im * s_re) + drive_im[row, :]
+        states[row, :128] = n_re
+        states[row, 128:] = n_im
+        return n_re, n_im
+
+    lax.fori_loop(0, TOKENS, record, (carried[0], carried[1]), unroll=8)
+
+    def read(k, _):
+        at = pl.ds(pl.multiple_of(k * 256, 256), 256)
+        product = lax.dot_general(
+            states[at, :].astype(jnp.bfloat16),
+            read_w[...],
+            (((1,), (1,)), ((), ())),
+            preferred_element_type=jnp.float32,
+        )
+        drive_re[at, :] = product[:, :128]
+        drive_im[at, :] = product[:, 128:]
+        return 0
+
+    lax.fori_loop(0, 8, read, 0)
+    lane = lax.broadcasted_iota(jnp.int32, (TOKENS, 128), 1)
+    for side, buf in ((0, drive_re), (1, drive_im)):
+        picked = jnp.zeros((TOKENS, 128), jnp.float32)
+        for j in range(4):
+            value = buf[pl.ds(side * 4 + j, TOKENS, stride=8), :]
+            picked = jnp.where(lax.div(lane, 32) == j, value, picked)
+        skip = jnp.concatenate([skip_ref[g : g + 1, :] for g in range(side * 8, side * 8 + 8)], axis=1)
+        lanes = slice(side * 128, side * 128 + 128)
+        read_out = picked + skip * x_ref[:, lanes].astype(jnp.float32)
+        mixed[:, lanes] = jax.nn.gelu(read_out).astype(jnp.bfloat16)
+
+    def tp_copy(k):
+        peer = lax.rem(tp + k, TP)
+        rows = pl.ds(pl.multiple_of(peer * ROWS, ROWS), ROWS)
+        return remote(mixed.at[rows, :], whole.at[tp], tp_send.at[k], tp_recv.at[tp], tp=peer)
+
+    def send_tp(k, _):
+        tp_copy(k).start()
+        return 0
+
+    def tp_arrived(k, _):
+        source = lax.rem(tp + k, TP)
+        rows = pl.ds(pl.multiple_of(tp * ROWS, ROWS), ROWS)
+        remote(mixed.at[rows, :], whole.at[source], tp_send.at[k], tp_recv.at[source], tp=source).wait_recv()
+        return 0
+
+    lax.fori_loop(1, TP, send_tp, 0)
+    whole[tp] = mixed[pl.ds(pl.multiple_of(tp * ROWS, ROWS), ROWS), :]
 
     def twin_copy(block, piece, slot):
         return remote(
@@ -447,97 +515,20 @@
     twin_right_hi = twin_copy(right, piece_hi, 1)
     twin_left_lo.start()
     twin_right_hi.start()
-
-    lax.fori_loop(0, plane, column_arrived, 0)
-
-    def join_plane(p, carried):
-        return join(column_buf, p, carried, plane_re, plane_im)
-
-    carried = lax.fori_loop(0, plane, join_plane, (zero, zero, one))
-    carried = lax.fori_loop(0, place, join_place, carried)
-
-    def record(t, carried):
-        s_re, s_im = carried
-        row = pl.ds(pl.multiple_of(t * 8, 8), 8)
-        shr = shrink[row, :]
-        a_re = shr * keep_re
-        a_im = shr * keep_im
-        n_re = (a_re * s_re - a_im * s_im) + drive_re[row, :]
-        n_im = (a_re * s_im + a_im * s_re) + drive_im[row, :]
-        states[row, :128] = n_re
-        states[row, 128:] = n_im
-        return n_re, n_im
-
-    lax.fori_loop(0, TOKENS, record, (carried[0], carried[1]), unroll=8)
-
-    def read(k, _):
-        at = pl.ds(pl.multiple_of(k * 256, 256), 256)
-        product = lax.dot_general(
-            states[at, :].astype(jnp.bfloat16),
-            read_w[...],
-            (((1,), (1,)), ((), ())),
-            preferred_element_type=jnp.float32,
-        )
-        drive_re[at, :] = product[:, :128]
-        drive_im[at, :] = product[:, 128:]
-        return 0
-
-    lax.fori_loop(0, 8, read, 0)
-    lane = lax.broadcasted_iota(jnp.int32, (TOKENS, 128), 1)
-    for side, buf in ((0, drive_re), (1, drive_im)):
-        picked = jnp.zeros((TOKENS, 128), jnp.float32)
-        for j in range(4):
-            value = buf[pl.ds(side * 4 + j, TOKENS, stride=8), :]
-            picked = jnp.where(lax.div(lane, 32) == j, value, picked)
-        skip = jnp.concatenate([skip_ref[g : g + 1, :] for g in range(side * 8, side * 8 + 8)], axis=1)
-        lanes = slice(side * 128, side * 128 + 128)
-        read_out = picked + skip * x_ref[:, lanes].astype(jnp.float32)
-        mixed[:, lanes] = jax.nn.gelu(read_out).astype(jnp.bfloat16)
-
-    def tp_copy(k):
-        peer = lax.rem(tp + k, TP)
-        rows = pl.ds(pl.multiple_of(peer * ROWS, ROWS), ROWS)
-        return remote(mixed.at[rows, :], whole.at[tp], tp_send.at[k], tp_recv.at[tp], tp=peer)
-
-    def send_tp(k, _):
-        tp_copy(k).start()
-        return 0
-
-    def tp_arrived(k, _):
-        source = lax.rem(tp + k, TP)
-        rows = pl.ds(pl.multiple_of(tp * ROWS, ROWS), ROWS)
-        remote(mixed.at[rows, :], whole.at[source], tp_send.at[k], tp_recv.at[source], tp=source).wait_recv()
-        return 0
-
-    lax.fori_loop(1, TP, send_tp, 0)
-    whole[tp] = mixed[pl.ds(pl.multiple_of(tp * ROWS, ROWS), ROWS), :]
-
     from_left_hi.wait_recv()
     from_right_lo.wait_recv()
     twin_left_hi = twin_copy(left, piece_hi, 2)
     twin_right_lo = twin_copy(right, piece_lo, 3)
     twin_left_hi.start()
     twin_right_lo.start()
-    across_lo = ring(across, piece_lo, 0, 4)
-    across_hi = ring(across, piece_hi, 1, 5)
-    across_lo.wait_recv()
-    twin_across_lo = twin_copy(across, piece_lo, 4)
-    twin_across_lo.start()
-    across_hi.wait_recv()
-    twin_across_hi = twin_copy(across, piece_hi, 5)
-    twin_across_hi.start()
-
-    other = 2 * PIECE - half
-    other_lo = pl.ds(pl.multiple_of(other, PIECE), PIECE)
-    other_hi = pl.ds(pl.multiple_of(other + PIECE, PIECE), PIECE)
+
     lax.fori_loop(1, TP, tp_arrived, 0)
 
-    for p in (4, 3, 5, 2):
-        q = p - FAR // PLANE
+    for p in (3, 5, 2, 6):
         for piece in range(TP):
             lanes = slice(piece * 256, (piece + 1) * 256)
-            mixed_out[q * PLANE : (q + 1) * PLANE, :, lanes] = blocks(p, whole[piece])
-        lax.fori_loop(q * PLANE, (q + 1) * PLANE, send_mixed, 0)
+            mixed_out[p * PLANE : (p + 1) * PLANE, :, lanes] = blocks(p, whole[piece])
+        lax.fori_loop(p * PLANE, (p + 1) * PLANE, send_mixed, 0)
 
     def hidden_of(pieces, residual_rows):
         squares = jnp.zeros((ROWS, 1), jnp.float32)
@@ -551,6 +542,18 @@
         mix = deep_alpha * residual_rows.astype(jnp.float32) + mix * inverse
         return layer_norm(mix, mix_gain_ref[...]).astype(jnp.bfloat16)
 
+    across_lo = ring(across, piece_lo, 0, 4)
+    across_hi = ring(across, piece_hi, 1, 5)
+    across_lo.wait_recv()
+    twin_across_lo = twin_copy(across, piece_lo, 4)
+    twin_across_lo.start()
+    across_hi.wait_recv()
+    twin_across_hi = twin_copy(across, piece_hi, 5)
+    twin_across_hi.start()
+
+    other = 2 * PIECE - half
+    other_lo = pl.ds(pl.multiple_of(other, PIECE), PIECE)
+    other_hi = pl.ds(pl.multiple_of(other + PIECE, PIECE), PIECE)
     for slot, (block, piece) in enumerate(
         (
             (left, other_lo),
@@ -564,7 +567,7 @@
         twin_copy(block, piece, slot).wait_recv()
     hidden_buf[...] = hidden_of([whole[q] for q in range(TP)], residual_ref[...])
 
-    for p in (6, 1, 7, 0):
+    for p in (4, 1, 7, 0):
         outgoing[p * PLANE : (p + 1) * PLANE] = blocks(p, hidden_buf[...])
         lax.fori_loop(p * PLANE + (p == 0), (p + 1) * PLANE, send_out, 0)
     arrived[0] = outgoing[0]
@@ -578,9 +581,7 @@
             [buf[pl.ds(far, PLANE)].reshape(size, -1), buf[pl.ds(near, PLANE)].reshape(size, -1)], axis=0
         )
 
-    def expert(c, is_far):
-        far = (PLANES // 2 + c) * PLANE
-        near = (PLANES // 2 - 1 - c) * PLANE
+    def expert(far, near, is_far):
         near_first = jnp.maximum(near, 1)
 
         def out_arrived(k, _):
@@ -599,9 +600,9 @@
         lax.fori_loop(near_first, near + PLANE, out_arrived, 0)
         rows = rows_of(arrived, far, near)
         if is_far:
-            lax.fori_loop(far - FAR, far - FAR + PLANE, mixed_arrived, 0)
-            lax.fori_loop(near - FAR, near - FAR + PLANE, mixed_arrived, 0)
-            mixed_rows = rows_of(mixed_in, far - FAR, near - FAR)
+            lax.fori_loop(far, far + PLANE, mixed_arrived, 0)
+            lax.fori_loop(near, near + PLANE, mixed_arrived, 0)
+            mixed_rows = rows_of(mixed_in, far, near)
             rows = hidden_of([mixed_rows[:, q * 256 : (q + 1) * 256] for q in range(TP)], rows)
         gate_act = jnp.dot(rows, gate[...], preferred_element_type=jnp.float32)
         up_act = jnp.dot(rows, up[...], preferred_element_type=jnp.float32)
@@ -613,16 +614,49 @@
         lax.fori_loop(near_first, near + PLANE, send_back, 0)
 
     def far_expert(c, _):
-        expert(c, True)
+        expert((5 + c) * PLANE, (3 - c) * PLANE, True)
         return 0
 
     def near_expert(c, _):
-        expert(c, False)
+        expert((4 + 3 * c) * PLANE, c * PLANE, False)
         return 0
 
     lax.fori_loop(0, 2, far_expert, 0)
-    lax.fori_loop(2, 4, near_expert, 0)
+    lax.fori_loop(0, 2, near_expert, 0)
     returned[0] = produced[0]
+
+    def out_left(k, _):
+        out_copy(k).wait_send()
+        back_copy(k).wait_send()
+        return 0
+
+    def mixed_left(k, _):
+        mixed_copy(k).wait_send()
+        return 0
+
+    lax.fori_loop(1, EXPERTS, out_left, 0)
+    for p in (2, 3, 5, 6):
+        lax.fori_loop(p * PLANE, (p + 1) * PLANE, mixed_left, 0)
+
+    def plane_left(k, _):
+        plane_copy(k).wait_send()
+        return 0
+
+    def column_left(p, _):
+        column_copy(p).wait_send()
+        return 0
+
+    def tp_left(k, _):
+        tp_copy(k).wait_send()
+        return 0
+
+    lax.fori_loop(1, PLANE, plane_left, 0)
+    lax.fori_loop(plane + 1, PLANES, column_left, 0)
+    lax.fori_loop(1, TP, tp_left, 0)
+    for copy in (to_right_lo, to_left_hi, to_right_hi, to_left_lo, pass_right, pass_left):
+        copy.wait_send()
+    for copy in (twin_left_lo, twin_right_hi, twin_left_hi, twin_right_lo, twin_across_lo, twin_across_hi):
+        copy.wait_send()
 
     def back_arrived(k, _):
         back_copy(k).wait_recv()
@@ -635,38 +669,6 @@
     expert_mix = both[:ROWS] + both[ROWS:]
     final = layer_norm(deep_alpha * hidden_buf[...].astype(jnp.float32) + expert_mix, final_gain_ref[...])
     layer_ref[...] = final.astype(jnp.bfloat16)
-
-    def out_left(k, _):
-        out_copy(k).wait_send()
-        back_copy(k).wait_send()
-        return 0
-
-    def mixed_left(k, _):
-        mixed_copy(k).wait_send()
-        return 0
-
-    lax.fori_loop(1, EXPERTS, out_left, 0)
-    lax.fori_loop(0, FAR_BLOCKS, mixed_left, 0)
-
-    def plane_left(k, _):
-        plane_copy(k).wait_send()
-        return 0
-
-    def column_left(p, _):
-        column_copy(p).wait_send()
-        return 0
-
-    def tp_left(k, _):
-        tp_copy(k).wait_send()
-        return 0
-
-    lax.fori_loop(1, PLANE, plane_left, 0)
-    lax.fori_loop(plane + 1, PLANES, column_left, 0)
-    lax.fori_loop(1, TP, tp_left, 0)
-    for copy in (to_right_lo, to_left_hi, to_right_hi, to_left_lo, pass_right, pass_left):
-        copy.wait_send()
-    for copy in (twin_left_lo, twin_right_hi, twin_left_hi, twin_right_lo, twin_across_lo, twin_across_hi):
-        copy.wait_send()
 
 
 def local(
@@ -742,8 +744,8 @@
             pltpu.VMEM((ROWS, WIDTH), bf16),
             pltpu.VMEM((2 * ROWS, SLOTS), bf16),
             pltpu.VMEM((SLOTS, ROWS), bf16),
-            pltpu.VMEM((FAR_BLOCKS, CAPACITY, MIX_WIDTH), bf16),
-            pltpu.VMEM((FAR_BLOCKS, CAPACITY, MIX_WIDTH), bf16),
+            pltpu.VMEM((EXPERTS, CAPACITY, MIX_WIDTH), bf16),
+            pltpu.VMEM((EXPERTS, CAPACITY, MIX_WIDTH), bf16),
             pltpu.VMEM((EXPERTS, CAPACITY, WIDTH), bf16),
             pltpu.VMEM((EXPERTS, CAPACITY, WIDTH), bf16),
             pltpu.VMEM((EXPERTS, CAPACITY, WIDTH), bf16),
@@ -764,8 +766,8 @@
             dma((EXPERTS,)),
             dma((EXPERTS,)),
             dma((EXPERTS,)),
-            dma((FAR_BLOCKS,)),
-            dma((FAR_BLOCKS,)),
+            dma((EXPERTS,)),
+            dma((EXPERTS,)),
         ],
         compiler_params=pltpu.CompilerParams(
             collective_id=0, has_side_effects=True, vmem_limit_bytes=62 * 1024 * 1024

time: 85.1 us -> 79.2 us (0.931)
  Pallas kernels: 83.3 us -> 77.4 us
    pallas_call x1, Pallas kernels: 83.3 us -> 77.4 us  [local(): pl.pallas_call(layer_kernel, out_shape=jax.ShapeDtypeStruct((ROWS, WIDTH)...]
where the time goes in v4:
time: 79.2 us; the launch traced here: 79.1 us
  Pallas kernels  77.4 us (98%)
  local copies, waits for them, and re-layouts  1.67 us (2%)
    pallas_call x1, Pallas kernels, local(): pl.pallas_call(layer_kernel, out_shape=jax.ShapeDtypeStruct((ROWS, WIDTH)...  77.4 us
    unnamed x1, local copies, waits for them, and re-layouts  1.67 us

profile of v4, /device:TPU:1, one launch (start us, length us, event | category | flops | bytes accessed | tf_op | source)
XLA Modules:
  0.0 79.1 jit_solution(3161186648878228448)
XLA Ops:
  0.0 77.4 %layer.1 = bf16[64,2048]{1,0:T(8,128)(2,1)} custom-call(f32[16]{0:T(128)} %step_ref.1, bf16[256,256]{1,0:T(8,128)(2,1)} %x_hbm.1, f32[16,256]{1,0:T(8,128)} %ret_hbm.1, f32[16,64]{1,0:T(8,128)} %real_hbm.1, f32[16,64]{1,0:T(8,128)} %freq_hbm.1, f32[16,16,64]{2,1,0:T(8,128)} %bitcast.7, f32[16,16,64]{2,1,0:T(8,128)} %bitcast.8, f32[16,16,64]{2,1,0:T(8,128)} %out_real_hbm.1, ...), custom_call_target="tpu_custom_call" | custom-call | tf_op jit(solution)/shard_map/layer/pallas_call | solution.py:720
  77.4 1.7 %copy.22 = bf16[64,2048]{1,0:T(8,128)(2,1)} copy(bf16[64,2048]{1,0:T(8,128)(2,1)} %layer.1) | data formatting | bytes 524288

commit v5 on v4

--- a/solution.py
+++ b/solution.py
@@ -451,7 +451,7 @@
     lax.fori_loop(0, TOKENS, record, (carried[0], carried[1]), unroll=8)
 
     def read(k, _):
-        at = pl.ds(pl.multiple_of(k * 256, 256), 256)
+        at = pl.ds(pl.multiple_of(k * 1024, 1024), 1024)
         product = lax.dot_general(
             states[at, :].astype(jnp.bfloat16),
             read_w[...],
@@ -462,7 +462,7 @@
         drive_im[at, :] = product[:, 128:]
         return 0
 
-    lax.fori_loop(0, 8, read, 0)
+    lax.fori_loop(0, 2, read, 0)
     lane = lax.broadcasted_iota(jnp.int32, (TOKENS, 128), 1)
     for side, buf in ((0, drive_re), (1, drive_im)):
         picked = jnp.zeros((TOKENS, 128), jnp.float32)
@@ -719,7 +719,7 @@
     large = (projection, expert_gate, expert_up, expert_down)
     return pl.pallas_call(
         layer_kernel,
-        out_shape=jax.ShapeDtypeStruct((ROWS, WIDTH), bf16),
+        out_shape=pltpu.VMEM((ROWS, WIDTH), bf16),
         in_specs=[smem] + [hbm] * (len(small) + len(large)),
         out_specs=vmem,
         scratch_shapes=[pltpu.VMEM(a.shape, a.dtype) for a in small]

time: 79.2 us -> 77.2 us (0.975)
  Pallas kernels: 77.4 us -> 76.3 us
  local copies, waits for them, and re-layouts: 1.67 us -> 0.71 us
    pallas_call x1, Pallas kernels: 77.4 us -> 76.3 us  [local(): pl.pallas_call(layer_kernel, out_shape=pltpu.VMEM((ROWS, WIDTH), bf16), i...]
    unnamed x1, local copies, waits for them, and re-layouts: 1.67 us -> 0.71 us
where the time goes in v5:
time: 77.2 us; the launch traced here: 77 us
  Pallas kernels  76.3 us (99%)
    pallas_call x1, Pallas kernels, local(): pl.pallas_call(layer_kernel, out_shape=pltpu.VMEM((ROWS, WIDTH), bf16), i...  76.3 us

profile of v5, /device:TPU:1, one launch (start us, length us, event | category | flops | bytes accessed | tf_op | source)
XLA Modules:
  0.0 77.0 jit_solution(11960266016478303069)
XLA Ops:
  0.0 76.3 %layer.1 = bf16[64,2048]{1,0:T(8,128)(2,1)S(1)} custom-call(f32[16]{0:T(128)} %step_ref.1, bf16[256,256]{1,0:T(8,128)(2,1)} %x_hbm.1, f32[16,256]{1,0:T(8,128)} %ret_hbm.1, f32[16,64]{1,0:T(8,128)} %real_hbm.1, f32[16,64]{1,0:T(8,128)} %freq_hbm.1, f32[16,16,64]{2,1,0:T(8,128)} %bitcast.7, f32[16,16,64]{2,1,0:T(8,128)} %bitcast.8, ...), custom_call_target="tpu_custom_call" | custom-call | tf_op jit(solution)/shard_map/layer/pallas_call | solution.py:720
  76.3 0.7 copy.22

commit v6 on v5

--- a/solution.py
+++ b/solution.py
@@ -146,30 +146,7 @@
     left = lax.rem(tp + TP - 1, TP)
     across = lax.rem(tp + 2, TP)
 
-    barrier = pltpu.get_barrier_semaphore()
-
-    def greet_plane(k, _):
-        peer = plane * PLANE + lax.rem(place + k, PLANE)
-        pl.semaphore_signal(barrier, inc=1, device_id={"sp": peer}, device_id_type=MESH)
-        return 0
-
-    def greet_column(k, _):
-        peer = lax.rem(plane + k, PLANES) * PLANE + place
-        pl.semaphore_signal(barrier, inc=1, device_id={"sp": peer}, device_id_type=MESH)
-        return 0
-
-    def greet_tp(k, _):
-        pl.semaphore_signal(
-            barrier, inc=1, device_id={"tp": lax.rem(tp + k, TP)}, device_id_type=MESH
-        )
-        return 0
-
-    lax.fori_loop(1, TP, greet_tp, 0)
-    lax.fori_loop(1, PLANE, greet_plane, 0)
-    lax.fori_loop(1, PLANES, greet_column, 0)
-
     own_copy = pltpu.make_async_copy(proj_ref, gathered.at[tp], own_sem)
-    own_copy.start()
     loads = [
         pltpu.make_async_copy(source, target, load_sem.at[k])
         for k, (source, target) in enumerate(
@@ -195,7 +172,33 @@
             )
         )
     ]
-    for load in loads:
+    for load in loads[:8]:
+        load.start()
+    own_copy.start()
+
+    barrier = pltpu.get_barrier_semaphore()
+
+    def greet_plane(k, _):
+        peer = plane * PLANE + lax.rem(place + k, PLANE)
+        pl.semaphore_signal(barrier, inc=1, device_id={"sp": peer}, device_id_type=MESH)
+        return 0
+
+    def greet_column(k, _):
+        peer = lax.rem(plane + k, PLANES) * PLANE + place
+        pl.semaphore_signal(barrier, inc=1, device_id={"sp": peer}, device_id_type=MESH)
+        return 0
+
+    def greet_tp(k, _):
+        pl.semaphore_signal(
+            barrier, inc=1, device_id={"tp": lax.rem(tp + k, TP)}, device_id_type=MESH
+        )
+        return 0
+
+    lax.fori_loop(1, TP, greet_tp, 0)
+    lax.fori_loop(1, PLANE, greet_plane, 0)
+    lax.fori_loop(1, PLANES, greet_column, 0)
+
+    for load in loads[8:]:
         load.start()
     for load in loads[:8]:
         load.wait()

time: 77.2 us -> 76.9 us (level)
  no operation moved by 1% of the time
where the time goes in v6:
time: 76.9 us; the launch traced here: 76.8 us
  Pallas kernels  76.1 us (99%)
    pallas_call x1, Pallas kernels, local(): pl.pallas_call(layer_kernel, out_shape=pltpu.VMEM((ROWS, WIDTH), bf16), i...  76.1 us

profile of v6, /device:TPU:1, one launch (start us, length us, event | category | flops | bytes accessed | tf_op | source)
XLA Modules:
  0.0 76.8 jit_solution(11501772314377889752)
XLA Ops:
  0.0 76.1 %layer.1 = bf16[64,2048]{1,0:T(8,128)(2,1)S(1)} custom-call(f32[16]{0:T(128)} %step_ref.1, bf16[256,256]{1,0:T(8,128)(2,1)} %x_hbm.1, f32[16,256]{1,0:T(8,128)} %ret_hbm.1, f32[16,64]{1,0:T(8,128)} %real_hbm.1, f32[16,64]{1,0:T(8,128)} %freq_hbm.1, f32[16,16,64]{2,1,0:T(8,128)} %bitcast.7, f32[16,16,64]{2,1,0:T(8,128)} %bitcast.8, ...), custom_call_target="tpu_custom_call" | custom-call | tf_op jit(solution)/shard_map/layer/pallas_call | solution.py:723
  76.1 0.7 copy.22

commit v7 on v6

--- a/solution.py
+++ b/solution.py
@@ -12,6 +12,7 @@
 deep_alpha = 2.0**0.25
 
 TOKENS = 256
+HALF = TOKENS // 2
 GROUPS = 16
 CHANNELS = 16
 STATE = 64
@@ -254,13 +255,11 @@
     rest = kept - kept_hi.astype(jnp.float32)
     kept_mid = rest.astype(jnp.bfloat16)
     kept_lo = (rest - kept_mid.astype(jnp.float32)).astype(jnp.bfloat16)
-    select_row = lax.broadcasted_iota(jnp.int32, (GROUPS, 8 * 128), 0)
-    select_lane = lax.broadcasted_iota(jnp.int32, (GROUPS, 8 * 128), 1)
-    select = (select_row == lax.div(select_lane, STATE)).astype(jnp.bfloat16)
-    spread = (
-        jnp.dot(kept_hi, select, preferred_element_type=jnp.float32)
-        + jnp.dot(kept_mid, select, preferred_element_type=jnp.float32)
-        + jnp.dot(kept_lo, select, preferred_element_type=jnp.float32)
+    select_row = lax.broadcasted_iota(jnp.int32, (3 * GROUPS, 8 * 128), 0)
+    select_lane = lax.broadcasted_iota(jnp.int32, (3 * GROUPS, 8 * 128), 1)
+    select = (lax.rem(select_row, GROUPS) == lax.div(select_lane, STATE)).astype(jnp.bfloat16)
+    spread = jnp.dot(
+        jnp.concatenate([kept_hi, kept_mid, kept_lo], axis=1), select, preferred_element_type=jnp.float32
     )
     x = x_ref[...]
     for j in range(8):
@@ -296,26 +295,36 @@
     to_right_hi.start()
     to_left_lo.start()
 
-    def advance(t, carried):
-        s_re, s_im, decay = carried
+    def step(t, s_re, s_im):
         row = pl.ds(pl.multiple_of(t * 8, 8), 8)
         shr = shrink[row, :]
         a_re = shr * keep_re
         a_im = shr * keep_im
         n_re = (a_re * s_re - a_im * s_im) + drive_re[row, :]
         n_im = (a_re * s_im + a_im * s_re) + drive_im[row, :]
-        return n_re, n_im, decay * shr
+        return n_re, n_im, shr, row
+
+    def advance(t, carried):
+        f_re, f_im, f_decay, s_re, s_im, s_decay = carried
+        f_re, f_im, f_shr, _ = step(t, f_re, f_im)
+        s_re, s_im, s_shr, _ = step(t + HALF, s_re, s_im)
+        return f_re, f_im, f_decay * f_shr, s_re, s_im, s_decay * s_shr
+
+    half_re, half_im = keep_re, keep_im
+    for _ in range(7):
+        half_re, half_im = times(half_re, half_im, half_re, half_im)
+    power_re, power_im = times(half_re, half_im, half_re, half_im)
 
     zero = jnp.zeros((8, 128), jnp.float32)
     one = jnp.ones((8, 128), jnp.float32)
-    end_re, end_im, decay = lax.fori_loop(0, TOKENS, advance, (zero, zero, one), unroll=8)
-    mine[0] = end_re
-    mine[1] = end_im
-    mine[2] = decay
-
-    power_re, power_im = keep_re, keep_im
-    for _ in range(8):
-        power_re, power_im = times(power_re, power_im, power_re, power_im)
+    first_re, first_im, first_decay, last_re, last_im, last_decay = lax.fori_loop(
+        0, HALF, advance, (zero, zero, one, zero, zero, one), unroll=8
+    )
+    end_re, end_im = times(last_decay * half_re, last_decay * half_im, first_re, first_im)
+    mine[0] = end_re + last_re
+    mine[1] = end_im + last_im
+    mine[2] = first_decay * last_decay
+
     plane_re, plane_im = power_re, power_im
     for _ in range(3):
         plane_re, plane_im = times(plane_re, plane_im, plane_re, plane_im)
@@ -440,18 +449,23 @@
     carried = lax.fori_loop(0, place, join_place, carried)
 
     def record(t, carried):
-        s_re, s_im = carried
-        row = pl.ds(pl.multiple_of(t * 8, 8), 8)
-        shr = shrink[row, :]
-        a_re = shr * keep_re
-        a_im = shr * keep_im
-        n_re = (a_re * s_re - a_im * s_im) + drive_re[row, :]
-        n_im = (a_re * s_im + a_im * s_re) + drive_im[row, :]
-        states[row, :128] = n_re
-        states[row, 128:] = n_im
-        return n_re, n_im
-
-    lax.fori_loop(0, TOKENS, record, (carried[0], carried[1]), unroll=8)
+        f_re, f_im, s_re, s_im = carried
+        f_re, f_im, _, row = step(t, f_re, f_im)
+        states[row, :128] = f_re
+        states[row, 128:] = f_im
+        s_re, s_im, _, row = step(t + HALF, s_re, s_im)
+        states[row, :128] = s_re
+        states[row, 128:] = s_im
+        return f_re, f_im, s_re, s_im
+
+    later_re, later_im = times(first_decay * half_re, first_decay * half_im, carried[0], carried[1])
+    lax.fori_loop(
+        0,
+        HALF,
+        record,
+        (carried[0], carried[1], later_re + first_re, later_im + first_im),
+        unroll=8,
+    )
 
     def read(k, _):
         at = pl.ds(pl.multiple_of(k * 1024, 1024), 1024)

time: 76.9 us -> 76.6 us (level)
  no operation moved by 1% of the time
where the time goes in v7:
time: 76.6 us; the launch traced here: 76.4 us
  Pallas kernels  75.7 us (99%)
    pallas_call x1, Pallas kernels, local(): pl.pallas_call(layer_kernel, out_shape=pltpu.VMEM((ROWS, WIDTH), bf16), i...  75.7 us

profile of v7, /device:TPU:1, one launch (start us, length us, event | category | flops | bytes accessed | tf_op | source)
XLA Modules:
  0.0 76.4 jit_solution(795906245752332070)
XLA Ops:
  0.0 75.7 %layer.1 = bf16[64,2048]{1,0:T(8,128)(2,1)S(1)} custom-call(f32[16]{0:T(128)} %step_ref.1, bf16[256,256]{1,0:T(8,128)(2,1)} %x_hbm.1, f32[16,256]{1,0:T(8,128)} %ret_hbm.1, f32[16,64]{1,0:T(8,128)} %real_hbm.1, f32[16,64]{1,0:T(8,128)} %freq_hbm.1, f32[16,16,64]{2,1,0:T(8,128)} %bitcast.7, f32[16,16,64]{2,1,0:T(8,128)} %bitcast.8, ...), custom_call_target="tpu_custom_call" | custom-call | tf_op jit(solution)/shard_map/layer/pallas_call | solution.py:737
  75.7 0.7 copy.22
